TPU v7x, 256 devices: a whole 4x4x8 slice. The times are simulated.
256 devices in a mesh: ep: 128 (over z, y, x), tp: 2 (over core).
Axes of the slice: x: 4, y: 4, z: 8, core: 2. Of those that a mesh axis runs over, the one named last changes fastest.
Arguments:
- tokens: bfloat16 [2048, 2048], P('ep'), may hold values from -6 to 6
- mix_gain: float32 [2048], replicated, may hold values from 0.1 to 1.9
- query_weight: bfloat16 [2048, 1024], P('ep', 'tp'), may hold values from -0.125 to 0.125
- forget_weight: bfloat16 [2048, 1024], P('ep', 'tp'), may hold values from -0.125 to 0.125
- input_weight: bfloat16 [2048, 1024], P('ep', 'tp'), may hold values from -0.125 to 0.125
- lower_bound: float32 [1024], P('tp'), may hold values from 0 to 0.9
- head_gain: float32 [1024], P('tp'), may hold values from 0.1 to 1.9
- out_weight: bfloat16 [1024, 2048], P('tp', 'ep'), may hold values from -0.1875 to 0.1875
- state: float32 [2048, 8, 128, 128], P('ep', 'tp'), may hold values from -4 to 4
- ffn_gain: float32 [2048], replicated, may hold values from 0.1 to 1.9
- route_ids: int32 [2048, 2], P('ep'), may hold values from 0 to 7, all different within a row; in each aligned block of 16 rows (0 to 15, 16 to 31, ...) at most 6 rows name the same one
- route_weights: float32 [2048, 2], P('ep'), may hold values from 0.25 to 1
- expert_gate: bfloat16 [128, 2048, 256], P('ep', None, 'tp'), may hold values from -0.125 to 0.125
- expert_up: bfloat16 [128, 2048, 256], P('ep', None, 'tp'), may hold values from -0.125 to 0.125
- expert_down: bfloat16 [128, 256, 2048], P('ep', 'tp'), may hold values from -0.09375 to 0.09375
Outputs:
- mixed_out: bfloat16 [2048, 2048], P('ep', 'tp')
- new_state: float32 [2048, 8, 128, 128], P('ep', 'tp')
Inputs may be any that keep to these rules, and one draw needn't show every extreme that they name: `route_ids`: each row names 2 different experts; among the rows of one device no expert is named by more than 6 rows, a bound that some block reaches of them.
All inputs are finite; a program needn't handle non-finite values.
Results may differ from a plain program's by a relative error of at most 0.015.
Values may be sent and summed in bfloat16 or wider, within the bound.
A program may use at most 64 MiB of HBM per device.

v0:
```python
import jax
import jax.numpy as jnp
from jax import lax
from jax.sharding import Mesh
from jax.sharding import PartitionSpec as P

EXPERTS = 8
TOP = 2
EP = ("ep_0", "ep_1", "ep_2")


epsilon = 1e-06


def side_by_side(arrays, axis, dim, along):
    both = jnp.concatenate(arrays, axis=along)
    filled, at, done = (lax.all_gather(both, axis, axis=dim, tiled=True), 0, [])
    for a in arrays:
        done.append(lax.slice_in_dim(filled, at, at + a.shape[along], axis=along))
        at += a.shape[along]
    return tuple(done)


def gathered_by_axis(shard, axes, dim):
    for axis in reversed(axes):
        shard = lax.all_gather(shard, axis, axis=dim, tiled=True)
    return shard


def sent_to_all(shard, axis):
    copies = jnp.broadcast_to(shard, (lax.axis_size(axis), *shard.shape))
    return lax.all_to_all(copies, axis, split_axis=0, concat_axis=0, tiled=True)


def over_copies(shard, axis):
    everything = sent_to_all(shard, axis)
    return jnp.sum(everything.astype(jnp.float32), axis=0)


def cut_along(shard, dim, peers):
    before, after = (shard.shape[:dim], shard.shape[dim + 1 :])
    return jnp.moveaxis(shard.reshape(*before, peers, -1, *after), dim, 0)


def summed_on_arrival(shard, axis, dim):
    parts = cut_along(shard, dim, lax.axis_size(axis))
    arrived = lax.all_to_all(parts, axis, split_axis=0, concat_axis=0, tiled=True)
    return arrived.astype(jnp.float32).sum(axis=0)


def rms_scale(values_in, gain_vec):
    return (
        values_in
        * lax.rsqrt(jnp.mean(values_in * values_in, axis=-1, keepdims=True) + epsilon)
        * gain_vec
    )


def slot_ranks(block_ids, expert_count):
    onehot = (block_ids[..., None] == jnp.arange(expert_count, dtype=jnp.int32)).astype(jnp.int32)
    before = jnp.cumsum(onehot, axis=1) - onehot
    return jnp.sum(before * onehot, axis=-1)


def shards(
    tokens,
    mix_gain,
    query_weight,
    forget_weight,
    input_weight,
    lower_bound,
    head_gain,
    out_weight,
    state,
    ffn_gain,
    route_ids,
    route_weights,
    expert_gate,
    expert_up,
    expert_down,
):
    seq_dev = tokens.shape[0]
    model_width = tokens.shape[1]
    ep_count = lax.axis_size(EP)
    residual = tokens.astype(jnp.float32)
    normed = rms_scale(residual, mix_gain).astype(jnp.bfloat16)
    head_count = state.shape[1]
    head_size = state.shape[2]
    proj_width = query_weight.shape[1]
    pieces = side_by_side((query_weight, forget_weight, input_weight), EP, 0, 1)
    queries, forget_pre, fresh_values = tuple(
        (jnp.dot(normed, weight_rows, preferred_element_type=jnp.float32) for weight_rows in pieces)
    )
    forget = (lower_bound + (1.0 - lower_bound) * jax.nn.sigmoid(forget_pre)).reshape(
        seq_dev, head_count, head_size
    )
    queries = queries.reshape(seq_dev, head_count, head_size)
    fresh_values = fresh_values.reshape(seq_dev, head_count, head_size)
    new_state = forget[..., None] * state + (1.0 - forget)[..., None] * fresh_values[:, :, None, :]
    readout = jnp.einsum("shk,shkv->shv", queries, new_state, precision=lax.Precision.HIGHEST)
    readout = rms_scale(readout, head_gain.reshape(head_count, head_size))
    heads_out = readout.reshape(seq_dev, proj_width).astype(jnp.bfloat16)
    partial_mix = jnp.dot(
        heads_out, gathered_by_axis(out_weight, EP, 1), preferred_element_type=jnp.float32
    )
    mixer_sum = over_copies(partial_mix.astype(jnp.bfloat16), "tp").astype(jnp.float32)
    after_mixer = (residual + mixer_sum).astype(jnp.bfloat16)
    ffn_in = rms_scale(after_mixer.astype(jnp.float32), ffn_gain).astype(jnp.bfloat16)
    capacity = 3 * seq_dev // 8
    expert_span = ep_count // EXPERTS
    half_width = model_width // lax.axis_size("tp")
    own_columns = lax.dynamic_slice_in_dim(
        after_mixer, lax.axis_index("tp") * half_width, half_width, 1
    ).astype(jnp.float32)
    gate_slice = expert_gate[0]
    up_slice = expert_up[0]
    down_slice = expert_down[0]
    slot_iota = jnp.arange(capacity, dtype=jnp.int32)
    own_rank = slot_ranks(route_ids.reshape(1, seq_dev * TOP), EXPERTS).reshape(seq_dev, TOP)
    expert_iota = jnp.arange(EXPERTS, dtype=jnp.int32)
    chosen = (route_ids[:, :, None, None] == expert_iota[None, None, :, None]) & (
        own_rank[:, :, None, None] == slot_iota[None, None, None, :]
    )
    dispatch = jnp.any(chosen, axis=1).astype(jnp.bfloat16)
    combine = jnp.sum(chosen.astype(jnp.float32) * route_weights[:, :, None, None], axis=1)
    outgoing = jnp.einsum(
        "tec,td->ecd", dispatch, ffn_in, preferred_element_type=jnp.float32
    ).astype(jnp.bfloat16)
    outgoing = jnp.broadcast_to(
        outgoing[:, None], (EXPERTS, expert_span, capacity, model_width)
    ).reshape(ep_count, capacity, model_width)
    slot_rows = lax.all_to_all(outgoing, EP, split_axis=0, concat_axis=0, tiled=True)
    gate_pre = jnp.einsum(
        "...d,df->...f", slot_rows, gate_slice, preferred_element_type=jnp.float32
    )
    up_pre = jnp.einsum("...d,df->...f", slot_rows, up_slice, preferred_element_type=jnp.float32)
    hidden = (jax.nn.silu(gate_pre) * up_pre).astype(jnp.bfloat16)
    partial_out = jnp.einsum(
        "...f,fd->...d", hidden, down_slice, preferred_element_type=jnp.float32
    )
    reduced = summed_on_arrival(partial_out.astype(jnp.bfloat16), "tp", 2)
    returned = lax.all_to_all(
        reduced.astype(jnp.bfloat16), EP, split_axis=0, concat_axis=0, tiled=True
    ).astype(reduced.dtype)
    expert_out = jnp.sum(returned.reshape(EXPERTS, expert_span, capacity, half_width), axis=1)
    expert_mix = jnp.einsum("tec,ecd->td", combine, expert_out, precision=lax.Precision.HIGHEST)
    mixed_out = (own_columns + expert_mix).astype(jnp.bfloat16)
    return (mixed_out, new_state)


def solution(mesh):
    finer = Mesh(mesh.devices.reshape(8, 4, 4, mesh.shape["tp"]), ("ep_0", "ep_1", "ep_2", "tp"))
    placed = (
        P(EP, None),
        P(),
        P(EP, "tp"),
        P(EP, "tp"),
        P(EP, "tp"),
        P("tp"),
        P("tp"),
        P("tp", EP),
        P(EP, "tp", None, None),
        P(),
        P(EP, None),
        P(EP, None),
        P(EP, None, "tp"),
        P(EP, None, "tp"),
        P(EP, "tp", None),
    )
    return jax.shard_map(
        shards,
        mesh=finer,
        in_specs=placed,
        out_specs=(P(EP, "tp"), P(EP, "tp", None, None)),
        check_vma=False,
    )
```

profile of v0, /device:TPU:1, one launch (start us, length us, event | category | flops | bytes accessed | tf_op | source)
XLA Modules:
  0.0 386.1 jit_solution(7543772229755426298)
XLA Ops:
  7.3 1.4 pad_maximum_fusion
  8.7 10.4 %all_gather.13 = bf16[512,64]{0,1:T(8,128)(2,1)S(1)} all-gather(bf16[512,16]{0,1:T(8,128)(2,1)} %param.22), channel_id=1, replica_groups=mesh['ep_0'=8,'ep_1'=4,'ep_2'=4,'tp'=2] {'ep_2'}, dimensions={1}, use_global_device_ids=true | all-gather | bytes 81920 | tf_op jit(solution)/shard_map/all_gather | solution.py:26
  19.1 10.6 %all_gather.14 = bf16[512,256]{0,1:T(8,128)(2,1)} all-gather(bf16[512,64]{0,1:T(8,128)(2,1)S(1)} %all_gather.13), channel_id=1, replica_groups=mesh['ep_0'=8,'ep_1'=4,'ep_2'=4,'tp'=2] {'ep_1'}, dimensions={1}, use_global_device_ids=true | all-gather | bytes 327680 | tf_op jit(solution)/shard_map/all_gather | solution.py:26
  29.7 0.8 copy.61
  30.7 0.2 select_reduce_fusion
  31.1 0.7 iota_compare_fusion.2
  31.8 1.0 fusion.52
  32.8 0.7 broadcast_subtract_fusion.1
  33.5 98.6 %all-gather.3.cloned.1.call-done = bf16[2048,1536]{1,0:T(8,128)(2,1)} async-done(((bf16[16,1536]{1,0:T(8,128)(2,1)}), bf16[2048,1536]{1,0:T(8,128)(2,1)}) %all-gather.3.cloned.1.call-update) | async-done | bytes 6291472 | tf_op jit(solution)/shard_map/all_gather | solution.py:17
  132.0 2.1 fusion.35
  134.2 2.1 fusion.4
  136.3 2.0 fusion.8
  138.3 4.4 %multiply_add_fusion = f32[16,4,128,128]{3,2,1,0:T(8,128)S(1)} fusion(f32[16,4,128,128]{3,2,1,0:T(8,128)} %param.23, f32[16,4,128]{2,1,0:T(4,128)S(1)} %mul.124, f32[16,4,128]{2,1,0:T(4,128)S(1)} %broadcast_subtract_fusion, f32[16,4,128]{2,1,0:T(4,128)S(1)} %mul.120), kind=kLoop, calls=%fused_computation.1 | loop fusion | flops 3145728 | bytes 8486912 | tf_op jit(solution)/shard_map/add | solution.py:99
  142.8 2.0 copy-done.1
  144.8 3.7 fusion.69
  148.6 22.3 %all-gather.5.cloned.1.call-done = bf16[512,2048]{0,1:T(8,128)(2,1)} async-done(((bf16[512,256]{0,1:T(8,128)(2,1)}), bf16[512,2048]{0,1:T(8,128)(2,1)}) %all-gather.5.cloned.1.call-update) | async-done | bytes 2097168 | tf_op jit(solution)/shard_map/all_gather | solution.py:26
  170.9 2.2 convolution_convert_fusion.2
  173.2 8.4 %all_to_all.20 = bf16[2,16,2048]{2,1,0:T(8,128)(2,1)S(1)} all-to-all(bf16[2,16,2048]{2,1,0:T(8,128)(2,1)S(1)} %broadcast_in_dim.4), channel_id=1, replica_groups=mesh['ep_0'=8,'ep_1'=4,'ep_2'=4,'tp'=2] {'tp'}, dimensions={0} | all-to-all | bytes 262144 | tf_op jit(solution)/shard_map/all_to_all | solution.py:32
  181.8 0.3 convolution_convert_fusion.1
  182.2 0.5 broadcast_in_dim.5
  182.7 105.2 %all_to_all.21 = bf16[128,6,2048]{2,1,0:T(8,128)(2,1)S(1)} all-to-all(bf16[128,6,2048]{2,1,0:T(8,128)(2,1)S(1)} %bitcast.46), channel_id=1, replica_groups=mesh['ep_0'=8,'ep_1'=4,'ep_2'=4,'tp'=2] {'ep_0','ep_1','ep_2'}, dimensions={0} | all-to-all | bytes 6291456 | tf_op jit(solution)/shard_map/all_to_all | solution.py:132
  287.8 1.9 copy-done.2
  289.8 3.4 fusion.2
  293.2 8.9 %convolution_convert_fusion = bf16[128,6,2048]{2,0,1:T(8,128)(2,1)} fusion(bf16[128,6,2048]{2,1,0:T(8,128)(2,1)} %copy-done.2, bf16[1,128,2048]{2,1,0:T(8,128)(2,1)S(1)} %copy-done, bf16[1,2048,128]{2,1,0:T(8,128)(2,1)S(1)} %copy-done.8, f32[128,6,128]{2,0,1:T(8,128)S(1)} %fusion.2), kind=kOutput, calls=%fused_computation.2 | convolution fusion | flops 807469056 | bytes 7733248 | tf_op jit(solution)/shard_map/...f,fd->...d/dot_general | solution.py:138
  302.1 2.3 copy.94
  304.4 9.8 %all_to_all.22 = bf16[2,128,6,1024]{3,1,2,0:T(8,128)(2,1)} all-to-all(bf16[2,128,6,1024]{3,1,2,0:T(8,128)(2,1)S(1)} %bitcast.47), channel_id=1, replica_groups=mesh['ep_0'=8,'ep_1'=4,'ep_2'=4,'tp'=2] {'tp'}, dimensions={0} | all-to-all | bytes 6291456 | tf_op jit(solution)/shard_map/all_to_all | solution.py:47
  314.3 2.9 reduce_sum.81
  317.1 2.2 copy.68
  319.4 8.4 %all-to-all-start.3 = ((bf16[128,6,1024]{2,1,0:T(8,128)(2,1)}), bf16[128,6,1024]{2,1,0:T(8,128)(2,1)S(1)}, u32[]{:S(2)}, u32[]{:S(2)}) async-start(bf16[128,6,1024]{2,1,0:T(8,128)(2,1)} %copy.68), calls=%async_computation.3 | async-start | bytes 4194304 | tf_op jit(solution)/shard_map/all_to_all | solution.py:142
  327.8 50.0 %all-to-all-done.3 = bf16[128,6,1024]{2,1,0:T(8,128)(2,1)S(1)} async-done(((bf16[128,6,1024]{2,1,0:T(8,128)(2,1)}), bf16[128,6,1024]{2,1,0:T(8,128)(2,1)S(1)}, u32[]{:S(2)}, u32[]{:S(2)}) %all-to-all-start.3) | async-done | bytes 1572896 | tf_op jit(solution)/shard_map/all_to_all | solution.py:142
  377.8 0.5 convert_reduce_fusion
  378.3 0.9 fusion.19
  (43 shorter events, 1.2 us)
Async XLA Ops:
  7.2 286.0 %copy-start = (bf16[1,128,2048]{2,1,0:T(8,128)(2,1)S(1)}, bf16[1,128,2048]{2,1,0:T(8,128)(2,1)}, u32[]{:S(2)}) copy-start(bf16[1,128,2048]{2,1,0:T(8,128)(2,1)} %param.29) | copy-start | bytes 1572868
  7.2 129.1 %copy-start.3 = (bf16[16,2048]{1,0:T(8,128)(2,1)S(1)}, bf16[16,2048]{1,0:T(8,128)(2,1)}, u32[]{:S(2)}) copy-start(bf16[16,2048]{1,0:T(8,128)(2,1)} %param.15) | copy-start | bytes 196612
  7.2 129.1 %copy-start.9 = (f32[2048]{0:T(1024)S(1)}, f32[2048]{0:T(1024)}, u32[]{:S(2)}) copy-start(f32[2048]{0:T(1024)} %param.16) | copy-start | bytes 24580
  7.2 124.8 %all-gather.3.cloned.1.call-start = ((), (), s32[]{:S(2)}) async-start(), calls=%async_computation.4 | async-start | bytes 6340608 | tf_op jit(solution)/shard_map/all_gather | solution.py:17
  8.7 162.2 %all-gather.5.cloned.1.call-start = ((), (), s32[]{:S(2)}) async-start(), calls=%async_computation.5 | async-start | bytes 2359296 | tf_op jit(solution)/shard_map/all_gather | solution.py:26
  142.7 2.0 copy-start.1
  142.7 5.8 %copy-start.5 = (f32[512]{0:T(512)S(1)}, f32[512]{0:T(512)}, u32[]{:S(2)}) copy-start(f32[512]{0:T(512)} %param.21) | copy-start | bytes 6148
  142.8 39.0 %copy-start.4 = (f32[2048]{0:T(1024)S(1)}, f32[2048]{0:T(1024)}, u32[]{:S(2)}) copy-start(f32[2048]{0:T(1024)} %param.24) | copy-start | bytes 24580
  182.7 107.1 %copy-start.7 = (bf16[1,2048,128]{2,1,0:T(8,128)(2,1)S(1)}, bf16[1,2048,128]{2,1,0:T(8,128)(2,1)}, u32[]{:S(2)}) copy-start(bf16[1,2048,128]{2,1,0:T(8,128)(2,1)} %param.27) | copy-start | bytes 1572868
  287.8 1.9 copy-start.2
  289.8 3.4 copy-start.8
  317.1 10.6 %copy-start.6 = (f32[16,2]{0,1:T(2,128)S(1)}, f32[16,2]{0,1:T(2,128)}, u32[]{:S(2)}) copy-start(f32[16,2]{0,1:T(2,128)} %param.26) | copy-start | bytes 388
  319.4 58.4 %all-to-all-start.3 = ((bf16[128,6,1024]{2,1,0:T(8,128)(2,1)}), bf16[128,6,1024]{2,1,0:T(8,128)(2,1)S(1)}, u32[]{:S(2)}, u32[]{:S(2)}) async-start(bf16[128,6,1024]{2,1,0:T(8,128)(2,1)} %copy.68), calls=%async_computation.3 | async-start | bytes 4194304 | tf_op jit(solution)/shard_map/all_to_all | solution.py:142
Sparse Core Ops, SparseCore 0:
  12.2 119.7 all-gather.2
  133.8 37.0 all-gather.4
where the time goes:
time: 389 us; the launch traced here: 386 us
  waiting for transfers between devices  171 us (44%)
  blocking collectives  144 us (37%)
  matrix products  25.5 us (7%)
  between operations  14.3 us (4%)
  other arithmetic  12.3 us (3%)
  local copies, waits for them, and re-layouts  10.2 us (3%)
  starting transfers between devices  8.43 us (2%)
    all_to_all x1, blocking collectives, shards(): lax.all_to_all(outgoing, EP, split_axis=0, concat_axis=0, tiled=True)  105 us
    all_gather x1, waiting for transfers between devices, side_by_side(): filled, at, done = (lax.all_gather(both, axis, axis=dim, tiled=True), 0, [])  98.6 us
    all_to_all x1, waiting for transfers between devices, shards(): lax.all_to_all(reduced.astype(jnp.bfloat16), EP, split_axis=0, concat_axi...  50 us
    all_gather x1, waiting for transfers between devices, gathered_by_axis(): shard = lax.all_gather(shard, axis, axis=dim, tiled=True)  22.3 us
    all_gather x2, blocking collectives, gathered_by_axis(): shard = lax.all_gather(shard, axis, axis=dim, tiled=True)  21 us
    all_to_all x1, blocking collectives, summed_on_arrival(): lax.all_to_all(parts, axis, split_axis=0, concat_axis=0, tiled=True)  9.84 us
    dot_general x1, matrix products, shards(): jnp.einsum('...f,fd->...d', hidden, down_slice, preferred_element_type=jn...  8.87 us
    all_to_all x1, blocking collectives, sent_to_all(): return lax.all_to_all(copies, axis, split_axis=0, concat_axis=0, tiled=True)  8.38 us
  transfers between devices with their start and end apart: 3, of which 3 were waited for; matrix products, arithmetic and copies ran while one was open for 5% of the time, Pallas kernels for 0%

commit v1 on v0

--- a/solution.py
+++ b/solution.py
@@ -1,15 +1,286 @@
+import functools
 import jax
 import jax.numpy as jnp
 from jax import lax
+from jax.experimental import pallas as pl
+from jax.experimental.pallas import tpu as pltpu
 from jax.sharding import Mesh
 from jax.sharding import PartitionSpec as P
 
 EXPERTS = 8
 TOP = 2
-EP = ("ep_0", "ep_1", "ep_2")
-
-
+EP = ("z", "y", "x")
+MESH_ID = pl.DeviceIdType.MESH
+F32 = jnp.float32
+BF16 = jnp.bfloat16
 epsilon = 1e-06
+
+
+def place():
+    c, z = lax.axis_index("tp"), lax.axis_index("z")
+    y, x = lax.axis_index("y"), lax.axis_index("x")
+    first = c == 0
+    return c, z, y, x, jnp.where(first, x, y), jnp.where(first, y, x)
+
+
+def plane_id(c, u, v):
+    first = c == 0
+    return {"x": jnp.where(first, u, v), "y": jnp.where(first, v, u)}
+
+
+def remote(src, dst, send, recv, device):
+    return pltpu.make_async_remote_copy(
+        src_ref=src, dst_ref=dst, send_sem=send, recv_sem=recv, device_id=device, device_id_type=MESH_ID
+    )
+
+
+def arrived(ref, sem):
+    pltpu.make_async_copy(ref, ref, sem).wait()
+
+
+def route_slots(ids_ref, wts_ref):
+    row = lax.broadcasted_iota(jnp.int32, (64, 16), 0)
+    expert, slot = row // 8, row % 8
+    pick0 = (jnp.broadcast_to(ids_ref[0:1, :], (64, 16)) == expert).astype(F32)
+    pick1 = (jnp.broadcast_to(ids_ref[1:2, :], (64, 16)) == expert).astype(F32)
+    pick = pick0 + pick1
+    earlier = (
+        lax.broadcasted_iota(jnp.int32, (16, 16), 0) < lax.broadcasted_iota(jnp.int32, (16, 16), 1)
+    ).astype(F32)
+    rank = jnp.dot(pick, earlier, preferred_element_type=F32)
+    chosen = jnp.where(rank == slot.astype(F32), pick, 0.0)
+    weight = pick0 * jnp.broadcast_to(wts_ref[0:1, :], (64, 16)) + pick1 * jnp.broadcast_to(wts_ref[1:2, :], (64, 16))
+    return chosen, chosen * weight
+
+
+def squeeze_rows():
+    to = lax.broadcasted_iota(jnp.int32, (24, 32), 0)
+    frm = lax.broadcasted_iota(jnp.int32, (24, 32), 1)
+    return (((to // 6) * 8 + to % 6) == frm).astype(BF16)
+
+
+def spread_rows():
+    to = lax.broadcasted_iota(jnp.int32, (32, 24), 0)
+    frm = lax.broadcasted_iota(jnp.int32, (32, 24), 1)
+    return (((frm // 6) * 8 + frm % 6) == to).astype(BF16)
+
+
+def moe_kernel(
+    am_ref, gain_ref, ids_ref, wts_ref, gate_ref, up_ref, down_ref, out_ref,
+    wgu, wd, disp, zr, xg, po, r1, ss, r2, ret, rb,
+    wsem, wsend, wrecv, dsend, drecv, gsend, grecv, psend, precv, ssend, srecv, tsend, trecv,
+):
+    c, z, y, x, u, v = place()
+    half = am_ref.shape[1] // 2
+    mine = lax.rem(z, 2) == c
+    other = 1 - c
+    bar = pltpu.get_barrier_semaphore()
+    peers = [{"tp": other}]
+    for k in range(1, 8):
+        zk = lax.rem(z + k, 8)
+        peers += [{"z": zk}, {"z": zk, "tp": other}]
+    for k in range(1, 4):
+        peers += [plane_id(c, lax.rem(u + k, 4), v), plane_id(c, u, lax.rem(v + k, 4))]
+    for device in peers:
+        pl.semaphore_signal(bar, inc=1, device_id=device, device_id_type=MESH_ID)
+    own = pl.ds(pl.multiple_of(c * 128, 128), 128)
+    own_up = pl.ds(pl.multiple_of(256 + c * 128, 128), 128)
+    local = [
+        pltpu.make_async_copy(gate_ref.at[0], wgu.at[:, own], wsem.at[0]),
+        pltpu.make_async_copy(up_ref.at[0], wgu.at[:, own_up], wsem.at[1]),
+        pltpu.make_async_copy(down_ref.at[0], wd.at[own, :], wsem.at[2]),
+    ]
+    for copy in local:
+        copy.start()
+    rows = am_ref[...].astype(F32)
+    scale = lax.rsqrt(jnp.mean(rows * rows, axis=-1, keepdims=True) + epsilon)
+    ffn_in = (rows * scale * gain_ref[...]).astype(BF16)
+    chosen, weight = route_slots(ids_ref, wts_ref)
+    slots = jnp.dot(chosen.astype(BF16), ffn_in, preferred_element_type=F32).astype(BF16)
+    disp[...] = slots.reshape(disp.shape)
+    pl.semaphore_wait(bar, len(peers))
+    swap = [
+        remote(gate_ref.at[0], wgu.at[:, own], wsend.at[0], wrecv.at[0], {"tp": other}),
+        remote(up_ref.at[0], wgu.at[:, own_up], wsend.at[1], wrecv.at[1], {"tp": other}),
+        remote(down_ref.at[0], wd.at[own, :], wsend.at[2], wrecv.at[2], {"tp": other}),
+    ]
+    sends = []
+    for k in (4, 3, 5, 2, 6, 1, 7):
+        e = lax.rem(z + k, 8)
+        copy = remote(disp.at[e], zr.at[z // 2], dsend.at[k], drecv.at[z // 2], {"z": e})
+
+        @pl.when(mine)
+        def _(copy=copy):
+            copy.start()
+
+    for copy in swap:
+        copy.start()
+    for k in range(4):
+
+        @pl.when(2 * k + c != z)
+        def _(k=k):
+            arrived(zr.at[k], drecv.at[k])
+
+    @pl.when(mine)
+    def _():
+        zr[z // 2] = disp[z]
+
+    packed = jnp.dot(squeeze_rows(), zr[...].reshape(32, 2 * half), preferred_element_type=F32).astype(BF16)
+    home = v * 4 + u
+    xg[home] = packed
+    number = 0
+
+    def share(block, device):
+        nonlocal number
+        copy = remote(xg.at[block], xg.at[block], gsend.at[number], grecv.at[block], device)
+        copy.start()
+        sends.append(copy)
+        number += 1
+
+    for k in (2, 1, 3):
+        share(home, plane_id(c, lax.rem(u + k, 4), v))
+    for k in (2, 1, 3):
+        share(home, plane_id(c, u, lax.rem(v + k, 4)))
+    for k in (1, 3, 2):
+        block = v * 4 + lax.rem(u + k, 4)
+        arrived(xg.at[block], grecv.at[block])
+        for j in (2, 1, 3):
+            share(block, plane_id(c, u, lax.rem(v + j, 4)))
+    for copy in local:
+        copy.wait()
+    for copy in swap:
+        copy.wait_recv()
+
+    def group(step, carry):
+        vv = lax.rem(v + step, 4)
+        base = pl.multiple_of(vv * 4, 4)
+
+        @pl.when(step > 0)
+        def _():
+            for j in range(4):
+                arrived(xg.at[base + j], grecv.at[base + j])
+
+        lhs = xg[pl.ds(base, 4)].reshape(96, 2 * half)
+        pre = jnp.dot(lhs, wgu[...], preferred_element_type=F32)
+        gate_pre, up_pre = pre[:, :256], pre[:, 256:]
+        hidden = (gate_pre / (1.0 + jnp.exp(-gate_pre)) * up_pre).astype(BF16)
+        part = jnp.dot(hidden, wd[...], preferred_element_type=F32).astype(BF16)
+        po[vv] = part.reshape(4, 24, 2 * half)
+
+        @pl.when(step > 0)
+        def _():
+            remote(po.at[vv], r1.at[v], psend.at[vv], precv.at[v], plane_id(c, u, vv)).start()
+
+        return carry
+
+    lax.fori_loop(0, 4, group, 0)
+    for k in (1, 3, 2):
+        vk = lax.rem(v + k, 4)
+        arrived(r1.at[vk], precv.at[vk])
+    for k in (2, 1, 3, 0):
+        uk = lax.rem(u + k, 4)
+        total = po[v, uk].astype(F32)
+        for j in (1, 2, 3):
+            total += r1[lax.rem(v + j, 4), uk].astype(F32)
+        if k:
+            ss[uk] = total.astype(BF16)
+            remote(ss.at[uk], r2.at[u], ssend.at[k], srecv.at[u], plane_id(c, uk, v)).start()
+    for k in (1, 3, 2):
+        uk = lax.rem(u + k, 4)
+        arrived(r2.at[uk], srecv.at[uk])
+        total += r2[uk].astype(F32)
+    ret[...] = (
+        jnp.dot(spread_rows(), total.astype(BF16), preferred_element_type=F32).astype(BF16).reshape(ret.shape)
+    )
+    for k in range(4):
+        zk = 2 * k + c
+        for t in range(2):
+            piece = ret.at[k, :, pl.ds(t * half, half)]
+            copy = remote(piece, rb.at[z], tsend.at[k, t], trecv.at[z], {"z": zk, "tp": t})
+
+            @pl.when(jnp.logical_or(zk != z, c != t))
+            def _(copy=copy):
+                copy.start()
+
+    @pl.when(mine)
+    def _():
+        rb[z] = ret[z // 2, :, pl.ds(pl.multiple_of(c * half, half), half)]
+
+    for k in (1, 7, 2, 6, 3, 5, 4):
+        e = lax.rem(z + k, 8)
+        arrived(rb.at[e], trecv.at[e])
+
+    @pl.when(jnp.logical_not(mine))
+    def _():
+        arrived(rb.at[z], trecv.at[z])
+
+    returned = rb[...].reshape(64, half)
+    upper = weight.astype(BF16)
+    lower = (weight - upper.astype(F32)).astype(BF16)
+    dims = (((0,), (0,)), ((), ()))
+    mix = lax.dot_general(upper, returned, dims, preferred_element_type=F32)
+    mix += lax.dot_general(lower, returned, dims, preferred_element_type=F32)
+    keep = am_ref[:, pl.ds(pl.multiple_of(c * half, half), half)].astype(F32)
+    out_ref[...] = (keep + mix).astype(BF16)
+    for k in (4, 3, 5, 2, 6, 1, 7):
+
+        @pl.when(mine)
+        def _(k=k):
+            arrived(disp.at[0], dsend.at[k])
+
+    for copy in swap:
+        copy.wait_send()
+    for copy in sends:
+        copy.wait_send()
+    for k in (1, 2, 3):
+        vk = lax.rem(v + k, 4)
+        arrived(po.at[vk], psend.at[vk])
+        arrived(ss.at[0], ssend.at[k])
+    for k in range(4):
+        for t in range(2):
+
+            @pl.when(jnp.logical_or(2 * k + c != z, c != t))
+            def _(k=k, t=t):
+                arrived(rb.at[0], tsend.at[k, t])
+
+
+def experts(after_mixer, ffn_gain, route_ids, route_weights, expert_gate, expert_up, expert_down):
+    rows, width = after_mixer.shape
+    half = width // 2
+    vmem = pl.BlockSpec(memory_space=pltpu.VMEM)
+    hbm = pl.BlockSpec(memory_space=pltpu.HBM)
+    dma = pltpu.SemaphoreType.DMA
+    return pl.pallas_call(
+        moe_kernel,
+        out_shape=jax.ShapeDtypeStruct((rows, half), BF16),
+        in_specs=[vmem, vmem, vmem, vmem, hbm, hbm, hbm],
+        out_specs=vmem,
+        scratch_shapes=[
+            pltpu.VMEM((width, 512), BF16),
+            pltpu.VMEM((256, width), BF16),
+            pltpu.VMEM((8, 8, width), BF16),
+            pltpu.VMEM((4, 8, width), BF16),
+            pltpu.VMEM((16, 24, width), BF16),
+            pltpu.VMEM((4, 4, 24, width), BF16),
+            pltpu.VMEM((4, 4, 24, width), BF16),
+            pltpu.VMEM((4, 24, width), BF16),
+            pltpu.VMEM((4, 24, width), BF16),
+            pltpu.VMEM((4, 8, width), BF16),
+            pltpu.VMEM((8, 8, half), BF16),
+            dma((3,)), dma((3,)), dma((3,)),
+            dma((8,)), dma((4,)),
+            dma((15,)), dma((16,)),
+            dma((4,)), dma((4,)),
+            dma((4,)), dma((4,)),
+            dma((4, 2)), dma((8,)),
+        ],
+        compiler_params=pltpu.CompilerParams(
+            collective_id=3, has_side_effects=True, vmem_limit_bytes=40 * 2**20
+        ),
+        name="experts",
+    )(
+        after_mixer, ffn_gain.reshape(1, -1), route_ids.T, route_weights.T, expert_gate, expert_up, expert_down
+    )
 
 
 def side_by_side(arrays, axis, dim, along):
@@ -54,12 +325,6 @@
         * lax.rsqrt(jnp.mean(values_in * values_in, axis=-1, keepdims=True) + epsilon)
         * gain_vec
     )
-
-
-def slot_ranks(block_ids, expert_count):
-    onehot = (block_ids[..., None] == jnp.arange(expert_count, dtype=jnp.int32)).astype(jnp.int32)
-    before = jnp.cumsum(onehot, axis=1) - onehot
-    return jnp.sum(before * onehot, axis=-1)
 
 
 def shards(
@@ -105,51 +370,12 @@
     )
     mixer_sum = over_copies(partial_mix.astype(jnp.bfloat16), "tp").astype(jnp.float32)
     after_mixer = (residual + mixer_sum).astype(jnp.bfloat16)
-    ffn_in = rms_scale(after_mixer.astype(jnp.float32), ffn_gain).astype(jnp.bfloat16)
-    capacity = 3 * seq_dev // 8
-    expert_span = ep_count // EXPERTS
-    half_width = model_width // lax.axis_size("tp")
-    own_columns = lax.dynamic_slice_in_dim(
-        after_mixer, lax.axis_index("tp") * half_width, half_width, 1
-    ).astype(jnp.float32)
-    gate_slice = expert_gate[0]
-    up_slice = expert_up[0]
-    down_slice = expert_down[0]
-    slot_iota = jnp.arange(capacity, dtype=jnp.int32)
-    own_rank = slot_ranks(route_ids.reshape(1, seq_dev * TOP), EXPERTS).reshape(seq_dev, TOP)
-    expert_iota = jnp.arange(EXPERTS, dtype=jnp.int32)
-    chosen = (route_ids[:, :, None, None] == expert_iota[None, None, :, None]) & (
-        own_rank[:, :, None, None] == slot_iota[None, None, None, :]
-    )
-    dispatch = jnp.any(chosen, axis=1).astype(jnp.bfloat16)
-    combine = jnp.sum(chosen.astype(jnp.float32) * route_weights[:, :, None, None], axis=1)
-    outgoing = jnp.einsum(
-        "tec,td->ecd", dispatch, ffn_in, preferred_element_type=jnp.float32
-    ).astype(jnp.bfloat16)
-    outgoing = jnp.broadcast_to(
-        outgoing[:, None], (EXPERTS, expert_span, capacity, model_width)
-    ).reshape(ep_count, capacity, model_width)
-    slot_rows = lax.all_to_all(outgoing, EP, split_axis=0, concat_axis=0, tiled=True)
-    gate_pre = jnp.einsum(
-        "...d,df->...f", slot_rows, gate_slice, preferred_element_type=jnp.float32
-    )
-    up_pre = jnp.einsum("...d,df->...f", slot_rows, up_slice, preferred_element_type=jnp.float32)
-    hidden = (jax.nn.silu(gate_pre) * up_pre).astype(jnp.bfloat16)
-    partial_out = jnp.einsum(
-        "...f,fd->...d", hidden, down_slice, preferred_element_type=jnp.float32
-    )
-    reduced = summed_on_arrival(partial_out.astype(jnp.bfloat16), "tp", 2)
-    returned = lax.all_to_all(
-        reduced.astype(jnp.bfloat16), EP, split_axis=0, concat_axis=0, tiled=True
-    ).astype(reduced.dtype)
-    expert_out = jnp.sum(returned.reshape(EXPERTS, expert_span, capacity, half_width), axis=1)
-    expert_mix = jnp.einsum("tec,ecd->td", combine, expert_out, precision=lax.Precision.HIGHEST)
-    mixed_out = (own_columns + expert_mix).astype(jnp.bfloat16)
+    mixed_out = experts(after_mixer, ffn_gain, route_ids, route_weights, expert_gate, expert_up, expert_down)
     return (mixed_out, new_state)
 
 
 def solution(mesh):
-    finer = Mesh(mesh.devices.reshape(8, 4, 4, mesh.shape["tp"]), ("ep_0", "ep_1", "ep_2", "tp"))
+    finer = Mesh(mesh.devices.reshape(8, 4, 4, mesh.shape["tp"]), ("z", "y", "x", "tp"))
     placed = (
         P(EP, None),
         P(),

time: 389 us -> 242 us (0.62)
  blocking collectives: 144 us -> 29.4 us
  Pallas kernels: 0 us -> 52.1 us
  waiting for transfers between devices: 171 us -> 123 us
  matrix products: 25.5 us -> 12 us
  starting transfers between devices: 8.43 us -> 0.08 us
  local copies, waits for them, and re-layouts: 10.2 us -> 2.71 us
  other arithmetic: 12.3 us -> 7.66 us
    all_to_all x2 -> x0, blocking collectives: 115 us -> none  [the longest x1 105 us: shards(): lax.all_to_all(outgoing, EP, split_axis=0, concat_axis=0, tiled=True)]
    pallas_call x0 -> x1, Pallas kernels: none -> 52.1 us  [experts(): pl.pallas_call(moe_kernel, out_shape=jax.ShapeDtypeStruct((rows, half), B...]
    all_to_all x1 -> x0, waiting for transfers between devices: 50 us -> none  [shards(): lax.all_to_all(reduced.astype(jnp.bfloat16), EP, split_axis=0, concat_axi...]
    dot_general x4 -> x0, matrix products: 13.5 us -> none  [the longest x1 8.87 us: shards(): jnp.einsum('...f,fd->...d', hidden, down_slice, preferred_element_type=jn...]
    all_to_all x1 -> x0, starting transfers between devices: 8.35 us -> none  [shards(): lax.all_to_all(reduced.astype(jnp.bfloat16), EP, split_axis=0, concat_axi...]
  transfers between devices with their start and end apart: 3 -> 2, of which waited for: 3 -> 2; matrix products, arithmetic and copies ran while one was open for 5% -> 7% of each run, Pallas kernels for 0% -> 0%
where the time goes in v1:
time: 242 us; the launch traced here: 241 us
  waiting for transfers between devices  123 us (51%)
  Pallas kernels  52.1 us (22%)
  blocking collectives  29.4 us (12%)
  between operations  14.3 us (6%)
  matrix products  12 us (5%)
  other arithmetic  7.66 us (3%)
  local copies, waits for them, and re-layouts  2.71 us (1%)
    all_gather x1, waiting for transfers between devices, side_by_side(): filled, at, done = (lax.all_gather(both, axis, axis=dim, tiled=True), 0, [])  101 us
    pallas_call x1, Pallas kernels, experts(): pl.pallas_call(moe_kernel, out_shape=jax.ShapeDtypeStruct((rows, half), B...  52.1 us
    all_gather x1, waiting for transfers between devices, gathered_by_axis(): shard = lax.all_gather(shard, axis, axis=dim, tiled=True)  22.3 us
    all_gather x2, blocking collectives, gathered_by_axis(): shard = lax.all_gather(shard, axis, axis=dim, tiled=True)  21 us
    all_to_all x1, blocking collectives, sent_to_all(): return lax.all_to_all(copies, axis, split_axis=0, concat_axis=0, tiled=True)  8.43 us
    dot_general x3, matrix products, shards(): jnp.dot(normed, weight_rows, preferred_element_type=jnp.float32)  6.16 us
  transfers between devices with their start and end apart: 2, of which 2 were waited for; matrix products, arithmetic and copies ran while one was open for 7% of the time, Pallas kernels for 0%

profile of v1, /device:TPU:1, one launch (start us, length us, event | category | flops | bytes accessed | tf_op | source)
XLA Modules:
  0.0 241.2 jit_solution(16773565697770005141)
XLA Ops:
  7.2 0.0 copy-start.7
  7.2 0.0 copy-start.9
  7.2 0.0 all-gather.3.cloned.1.call-start
  7.2 1.4 pad_maximum_fusion
  8.6 0.0 all-gather.3.cloned.1.call-update
  8.6 0.0 all-gather.5.cloned.1.call-start
  8.7 10.4 %all_gather.13 = bf16[512,64]{0,1:T(8,128)(2,1)S(1)} all-gather(bf16[512,16]{0,1:T(8,128)(2,1)} %param.22), channel_id=1, replica_groups=mesh['z'=8,'y'=4,'x'=4,'tp'=2] {'x'}, dimensions={1}, use_global_device_ids=true | all-gather | bytes 81920 | tf_op jit(solution)/shard_map/all_gather | solution.py:297
  19.0 10.6 %all_gather.14 = bf16[512,256]{0,1:T(8,128)(2,1)} all-gather(bf16[512,64]{0,1:T(8,128)(2,1)S(1)} %all_gather.13), channel_id=1, replica_groups=mesh['z'=8,'y'=4,'x'=4,'tp'=2] {'y'}, dimensions={1}, use_global_device_ids=true | all-gather | bytes 327680 | tf_op jit(solution)/shard_map/all_gather | solution.py:297
  29.7 0.0 all-gather.5.cloned.1.call-update
  29.7 1.0 fusion.24
  30.7 0.7 broadcast_subtract_fusion.1
  31.4 100.7 %all-gather.3.cloned.1.call-done = bf16[2048,1536]{1,0:T(8,128)(2,1)} async-done(((bf16[16,1536]{1,0:T(8,128)(2,1)}), bf16[2048,1536]{1,0:T(8,128)(2,1)}) %all-gather.3.cloned.1.call-update) | async-done | bytes 6291472 | tf_op jit(solution)/shard_map/all_gather | solution.py:288
  132.0 2.1 fusion.21
  134.1 2.1 fusion.4
  136.3 2.0 fusion
  138.3 4.4 %multiply_add_fusion = f32[16,4,128,128]{3,2,1,0:T(8,128)S(1)} fusion(f32[16,4,128,128]{3,2,1,0:T(8,128)} %param.23, f32[16,4,128]{2,1,0:T(4,128)S(1)} %mul.84, f32[16,4,128]{2,1,0:T(4,128)S(1)} %broadcast_subtract_fusion, f32[16,4,128]{2,1,0:T(4,128)S(1)} %mul.80), kind=kLoop, calls=%fused_computation | loop fusion | flops 3145728 | bytes 8486912 | tf_op jit(solution)/shard_map/add | solution.py:364
  142.7 0.0 copy-start.6
  142.7 0.0 copy-start.8
  142.7 0.0 copy-start
  142.7 0.0 copy-start.1
  142.7 0.0 copy-start.2
  142.8 0.0 copy-start.4
  142.8 0.0 copy-start.5
  142.8 2.0 copy-done.6
  144.8 3.6 %fusion.33 = f32[16,4,1,128]{3,2,1,0:T(1,128)S(1)} fusion(f32[16,4,128,1]{2,3,1,0:T(1,128)S(1)} %bitcast.19, f32[16,4,128,128]{3,2,1,0:T(8,128)S(1)} %multiply_add_fusion), kind=kOutput, calls=%fused_computation.31 | convolution fusion | flops 12582912 | bytes 4259840 | tf_op jit(solution)/shard_map/shk,shkv->shv/dot_general | solution.py:365
  148.4 0.1 multiply_reduce_fusion
  148.5 0.1 multiply_convert_fusion
  148.6 22.3 %all-gather.5.cloned.1.call-done = bf16[512,2048]{0,1:T(8,128)(2,1)} async-done(((bf16[512,256]{0,1:T(8,128)(2,1)}), bf16[512,2048]{0,1:T(8,128)(2,1)}) %all-gather.5.cloned.1.call-update) | async-done | bytes 2097168 | tf_op jit(solution)/shard_map/all_gather | solution.py:297
  170.9 2.2 convolution_convert_fusion
  173.1 8.4 %all_to_all.5 = bf16[2,16,2048]{2,1,0:T(8,128)(2,1)S(1)} all-to-all(bf16[2,16,2048]{2,1,0:T(8,128)(2,1)S(1)} %broadcast_in_dim.2), channel_id=1, replica_groups=mesh['z'=8,'y'=4,'x'=4,'tp'=2] {'tp'}, dimensions={0} | all-to-all | bytes 262144 | tf_op jit(solution)/shard_map/all_to_all | solution.py:303
  181.7 52.1 %experts.1 = bf16[16,1024]{1,0:T(8,128)(2,1)S(1)} custom-call(bf16[16,2048]{1,0:T(8,128)(2,1)S(1)} %fusion.27.am_ref, f32[1,2048]{1,0:T(1,128)S(1)} %bitcast.14, s32[2,16]{1,0:T(2,128)S(1)} %bitcast.15, f32[2,16]{1,0:T(2,128)S(1)} %bitcast.16, bf16[1,2048,128]{2,1,0:T(8,128)(2,1)S(1)} %copy-done, bf16[1,2048,128]{2,1,0:T(8,128)(2,1)S(1)} %copy-done.1, ...), custom_call_target="tpu_custom_call" | custom-call | tf_op jit(solution)/shard_map/experts/pallas_call | solution.py:253
  233.8 0.6 copy.29
  (19 shorter events, 0.2 us)
Async XLA Ops:
  7.2 129.1 %copy-start.7 = (bf16[16,2048]{1,0:T(8,128)(2,1)S(1)}, bf16[16,2048]{1,0:T(8,128)(2,1)}, u32[]{:S(2)}) copy-start(bf16[16,2048]{1,0:T(8,128)(2,1)} %param.15) | copy-start | bytes 196612
  7.2 129.1 %copy-start.9 = (f32[2048]{0:T(1024)S(1)}, f32[2048]{0:T(1024)}, u32[]{:S(2)}) copy-start(f32[2048]{0:T(1024)} %param.16) | copy-start | bytes 24580
  7.2 124.8 %all-gather.3.cloned.1.call-start = ((), (), s32[]{:S(2)}) async-start(), calls=%async_computation.1 | async-start | bytes 6340608 | tf_op jit(solution)/shard_map/all_gather | solution.py:288
  8.6 162.2 %all-gather.5.cloned.1.call-start = ((), (), s32[]{:S(2)}) async-start(), calls=%async_computation.2 | async-start | bytes 2359296 | tf_op jit(solution)/shard_map/all_gather | solution.py:297
  142.7 2.1 copy-start.6
  142.7 5.8 %copy-start.8 = (f32[512]{0:T(512)S(1)}, f32[512]{0:T(512)}, u32[]{:S(2)}) copy-start(f32[512]{0:T(512)} %param.21) | copy-start | bytes 6148
  142.7 38.9 %copy-start = (bf16[1,2048,128]{2,1,0:T(8,128)(2,1)S(1)}, bf16[1,2048,128]{2,1,0:T(8,128)(2,1)}, u32[]{:S(2)}) copy-start(bf16[1,2048,128]{2,1,0:T(8,128)(2,1)} %gate_ref.1) | copy-start | bytes 1572868
  142.7 38.9 %copy-start.1 = (bf16[1,2048,128]{2,1,0:T(8,128)(2,1)S(1)}, bf16[1,2048,128]{2,1,0:T(8,128)(2,1)}, u32[]{:S(2)}) copy-start(bf16[1,2048,128]{2,1,0:T(8,128)(2,1)} %up_ref.1) | copy-start | bytes 1572868
  142.7 38.9 %copy-start.2 = (bf16[1,128,2048]{2,1,0:T(8,128)(2,1)S(1)}, bf16[1,128,2048]{2,1,0:T(8,128)(2,1)}, u32[]{:S(2)}) copy-start(bf16[1,128,2048]{2,1,0:T(8,128)(2,1)} %down_ref.1) | copy-start | bytes 1572868
  142.8 38.9 %copy-start.3 = (f32[2048]{0:T(1024)S(1)}, f32[2048]{0:T(1024)}, u32[]{:S(2)}) copy-start(f32[2048]{0:T(1024)} %param.24) | copy-start | bytes 24580
  142.8 38.9 %copy-start.4 = (s32[16,2]{0,1:T(2,128)S(1)}, s32[16,2]{0,1:T(2,128)}, u32[]{:S(2)}) copy-start(s32[16,2]{0,1:T(2,128)} %param.25) | copy-start | bytes 388
  142.8 38.9 %copy-start.5 = (f32[16,2]{0,1:T(2,128)S(1)}, f32[16,2]{0,1:T(2,128)}, u32[]{:S(2)}) copy-start(f32[16,2]{0,1:T(2,128)} %param.26) | copy-start | bytes 388
Sparse Core Ops, SparseCore 0:
  12.2 119.7 all-gather.2
  133.8 37.0 all-gather.4

commit v2 on v1

v2 whole, which is shorter than its diff:
```python
import functools
import jax
import jax.numpy as jnp
from jax import lax
from jax.experimental import pallas as pl
from jax.experimental.pallas import tpu as pltpu
from jax.sharding import Mesh
from jax.sharding import PartitionSpec as P

EXPERTS = 8
TOP = 2
EP = ("z", "y", "x")
MESH_ID = pl.DeviceIdType.MESH
F32 = jnp.float32
BF16 = jnp.bfloat16
epsilon = 1e-06


def place():
    c, z = lax.axis_index("tp"), lax.axis_index("z")
    y, x = lax.axis_index("y"), lax.axis_index("x")
    first = c == 0
    return c, z, y, x, jnp.where(first, x, y), jnp.where(first, y, x)


def plane_id(c, u, v):
    first = c == 0
    return {"x": jnp.where(first, u, v), "y": jnp.where(first, v, u)}


def remote(src, dst, send, recv, device):
    return pltpu.make_async_remote_copy(
        src_ref=src, dst_ref=dst, send_sem=send, recv_sem=recv, device_id=device, device_id_type=MESH_ID
    )


def arrived(ref, sem):
    pltpu.make_async_copy(ref, ref, sem).wait()


def route_slots(ids_ref, wts_ref):
    row = lax.broadcasted_iota(jnp.int32, (64, 16), 0)
    expert, slot = row // 8, row % 8
    pick0 = (jnp.broadcast_to(ids_ref[0:1, :], (64, 16)) == expert).astype(F32)
    pick1 = (jnp.broadcast_to(ids_ref[1:2, :], (64, 16)) == expert).astype(F32)
    pick = pick0 + pick1
    earlier = (
        lax.broadcasted_iota(jnp.int32, (16, 16), 0) < lax.broadcasted_iota(jnp.int32, (16, 16), 1)
    ).astype(F32)
    rank = jnp.dot(pick, earlier, preferred_element_type=F32)
    chosen = jnp.where(rank == slot.astype(F32), pick, 0.0)
    weight = pick0 * jnp.broadcast_to(wts_ref[0:1, :], (64, 16)) + pick1 * jnp.broadcast_to(wts_ref[1:2, :], (64, 16))
    return chosen, chosen * weight


def squeeze_rows():
    to = lax.broadcasted_iota(jnp.int32, (24, 32), 0)
    frm = lax.broadcasted_iota(jnp.int32, (24, 32), 1)
    return (((to // 6) * 8 + to % 6) == frm).astype(BF16)


def spread_rows():
    to = lax.broadcasted_iota(jnp.int32, (32, 24), 0)
    frm = lax.broadcasted_iota(jnp.int32, (32, 24), 1)
    return (((frm // 6) * 8 + frm % 6) == to).astype(BF16)


def halves(left, right, odd):
    lane = lax.broadcasted_iota(jnp.int32, left.shape, 1)
    if odd:
        left = pltpu.roll(left, 64, 1)
    else:
        right = pltpu.roll(right, 64, 1)
    return jnp.where(lane < 64, left, right)


def layer_kernel(
    tok_hbm, mixg_hbm, qw_hbm, fw_hbm, iw_hbm, lb_hbm, hg_hbm, wo_hbm, st_hbm, ffng_hbm, ids_hbm, wts_hbm,
    gate_ref, up_ref, down_ref, out_ref, st,
    tok, mixg, lb, hg, ffng, ids_ref, wts_ref, wcat, wb, xs, xb, ob, qb, ro, ho, wob, hb, pb, mb, am_ref, chosen_ref, weight_ref,
    wgu, wd, disp, zr, xg, po, r1, ss, r2, ret, rb,
    lsem, qsem, stsem, wsend, wrecv, xsend, xrecv, osend, orecv, wozs, wozr, woxs, woxr, hsend, hrecv, msend, mrecv,
    lwsem, swsend, swrecv, dsend, drecv, gsend, grecv, psend, precv, ssend, srecv, tsend, trecv,
):
    c, z, y, x, u, v = place()
    half = out_ref.shape[1]
    mine = lax.rem(z, 2) == c
    other = 1 - c
    spot = y * 4 + x
    bar = pltpu.get_barrier_semaphore()
    peers = [{"tp": other}]
    for dz in range(8):
        zk = lax.rem(z + dz, 8)
        for dx in range(4):
            if dz or dx:
                peers.append({"z": zk, "x": lax.rem(x + dx, 4)})
        if dz:
            peers.append({"z": zk, "tp": other})
    for dy in range(1, 4):
        yk = lax.rem(y + dy, 4)
        for dx in range(4):
            peers.append({"y": yk, "x": lax.rem(x + dx, 4)})
        peers.append({"y": yk, "tp": other})
    for device in peers:
        pl.semaphore_signal(bar, inc=1, device_id=device, device_id_type=MESH_ID)
    loads = [
        pltpu.make_async_copy(a, b, lsem.at[i])
        for i, (a, b) in enumerate(
            ((tok_hbm, tok), (mixg_hbm, mixg), (lb_hbm, lb), (hg_hbm, hg), (ffng_hbm, ffng), (ids_hbm, ids_ref), (wts_hbm, wts_ref),
             (wo_hbm, wob.at[z, x]))
        )
    ]
    own = pl.ds(pl.multiple_of(c * 128, 128), 128)
    own_up = pl.ds(pl.multiple_of(256 + c * 128, 128), 128)
    pieces = []
    for i, w_hbm in enumerate((qw_hbm, fw_hbm, iw_hbm)):
        for h in range(4):
            pieces.append(
                pltpu.make_async_copy(w_hbm.at[:, pl.ds(h * 128, 128)], wcat.at[h, :, pl.ds(i * 128, 128)], qsem.at[i, h])
            )
    for copy in loads[:2] + pieces + loads[2:]:
        copy.start()
    local = [
        pltpu.make_async_copy(gate_ref.at[0], wgu.at[:, own], lwsem.at[0]),
        pltpu.make_async_copy(up_ref.at[0], wgu.at[:, own_up], lwsem.at[1]),
        pltpu.make_async_copy(down_ref.at[0], wd.at[own, :], lwsem.at[2]),
    ]
    state_in = pltpu.make_async_copy(st_hbm, st, stsem)
    state_in.start()
    for copy in local:
        copy.start()
    for copy in loads[:2]:
        copy.wait()
    tokens = tok[...].astype(F32)
    scale = lax.rsqrt(jnp.mean(tokens * tokens, axis=-1, keepdims=True) + epsilon)
    normed = tokens * scale * mixg[...]
    for yk in range(4):
        for j in range(4):
            a, b = 4 * j + yk // 2, 4 * j + 2 + yk // 2
            xs[yk, :, pl.ds(j * 128, 128)] = halves(
                normed[:, a * 128 : a * 128 + 128], normed[:, b * 128 : b * 128 + 128], yk % 2
            ).astype(BF16)
    for copy in pieces:
        copy.wait()
    pl.semaphore_wait(bar, len(peers))
    out = []
    for dz in (4, 3, 5, 2, 6, 1, 7, 0):
        for dx in (2, 1, 3, 0):
            if dz or dx:
                xk = lax.rem(x + dx, 4)
                out.append(remote(wcat.at[xk], wb.at[z, x], wsend.at[dz, dx], wrecv, {"z": lax.rem(z + dz, 8), "x": xk}))
    for dy in (2, 1, 3, 0):
        for dx in (2, 1, 3, 0):
            if dy or dx:
                yk = lax.rem(y + dy, 4)
                out.append(remote(xs.at[yk], xb.at[spot], xsend.at[dy, dx], xrecv, {"y": yk, "x": lax.rem(x + dx, 4)}))
    for copy in out:
        copy.start()
    wb[z, x] = wcat[x]
    xb[spot] = xs[y]
    for copy in loads[2:]:
        copy.wait()
    spread = []
    for k in (4, 3, 5, 2, 6, 1, 7):
        spread.append(remote(wob.at[z, x], wob.at[z, x], wozs.at[k], wozr, {"z": lax.rem(z + k, 8)}))
    for copy in spread:
        copy.start()
    swap = [
        remote(gate_ref.at[0], wgu.at[:, own], swsend.at[0], swrecv.at[0], {"tp": other}),
        remote(up_ref.at[0], wgu.at[:, own_up], swsend.at[1], swrecv.at[1], {"tp": other}),
        remote(down_ref.at[0], wd.at[own, :], swsend.at[2], swrecv.at[2], {"tp": other}),
    ]
    for copy in swap:
        copy.start()
    chosen, weight = route_slots(ids_ref, wts_ref)
    chosen_ref[...] = chosen.astype(BF16)
    weight_ref[...] = weight
    arrived(xb.at[pl.ds(0, 15)], xrecv)
    wbf = wb.reshape(32, 16, 384)
    arrived(wbf.at[pl.ds(0, 31)], wrecv)
    part = jnp.dot(xb[...].reshape(256, 512), wbf[...].reshape(512, 384), preferred_element_type=F32)
    ob[...] = part.astype(BF16).reshape(16, 16, 384)
    back = []
    for dy in (2, 1, 3, 0):
        for dx in (2, 1, 3, 0):
            if dy or dx:
                yk, xk = lax.rem(y + dy, 4), lax.rem(x + dx, 4)
                back.append(remote(ob.at[yk * 4 + xk], qb.at[spot], osend.at[dy, dx], orecv, {"y": yk, "x": xk}))
    for copy in back:
        copy.start()
    qb[spot] = ob[spot]
    arrived(xb.at[pl.ds(0, 7)], wozr)
    along = []
    for k in (2, 1, 3):
        along.append(remote(wob.at[:, x], wob.at[:, x], woxs.at[k], woxr, {"x": lax.rem(x + k, 4)}))
    for copy in along:
        copy.start()
    state_in.wait()
    arrived(qb.at[pl.ds(0, 15)], orecv)

    def head(h, carry):
        qfv = (
            qb[h].astype(F32) + qb[4 + h].astype(F32) + qb[8 + h].astype(F32) + qb[12 + h].astype(F32)
        )
        bound = lb[pl.ds(h, 1), :]
        forget = bound + (1.0 - bound) * (1.0 / (1.0 + jnp.exp(-qfv[:, 128:256])))
        fresh = qfv[:, 256:384]
        q_t = qfv[:, 0:128].T
        f_t = forget.T
        for s in range(16):
            f_col = jnp.broadcast_to(f_t[:, s : s + 1], (128, 128))
            q_col = jnp.broadcast_to(q_t[:, s : s + 1], (128, 128))
            row = fresh[s : s + 1, :]
            new = row + f_col * (st[s, h] - row)
            st[s, h] = new
            ro[s : s + 1, :] = jnp.sum(q_col * new, axis=0, keepdims=True)
        read = ro[...]
        read = read * lax.rsqrt(jnp.mean(read * read, axis=-1, keepdims=True) + epsilon) * hg[pl.ds(h, 1), :]
        ho[:, pl.ds(pl.multiple_of(h * 128, 128), 128)] = read.astype(BF16)
        return carry

    lax.fori_loop(0, 4, head, 0)
    ahead = []
    for k in (2, 1, 3):
        ahead.append(remote(ho, hb.at[y], hsend.at[k], hrecv, {"y": lax.rem(y + k, 4)}))
    for copy in ahead:
        copy.start()
    hb[y] = ho[...]
    arrived(wob.at[:, pl.ds(0, 3)], woxr)
    arrived(hb.at[pl.ds(0, 3)], hrecv)
    dims = (((1,), (1,)), ((), ()))
    mixed = lax.dot_general(
        hb[...].reshape(64, 512), wob[...].reshape(512, 512), dims, preferred_element_type=F32
    )
    pb[...] = mixed.astype(BF16).reshape(4, 16, 512)
    home_bound = []
    for k in (2, 1, 3, 0):
        yk = lax.rem(y + k, 4)
        for t in (0, 1):
            if k or t:
                device = {"y": yk, "tp": lax.rem(c + t, 2)}
                home_bound.append(remote(pb.at[yk], mb.at[c, y], msend.at[k, t], mrecv, device))
    for copy in home_bound:
        copy.start()
    mb[c, y] = pb[y]
    arrived(mb.reshape(8, 16, 512).at[pl.ds(0, 7)], mrecv)
    sums = [mb[0, k].astype(F32) + mb[1, k].astype(F32) for k in range(4)]
    for zk in range(8):
        at = (zk // 2) * 128
        for h in range(2):
            cols = pl.ds(zk * 256 + h * 128, 128)
            got = halves(sums[2 * h][:, at : at + 128], sums[2 * h + 1][:, at : at + 128], zk % 2)
            am_ref[:, cols] = (tok[:, cols].astype(F32) + got).astype(BF16)
    rows = am_ref[...].astype(F32)
    scale = lax.rsqrt(jnp.mean(rows * rows, axis=-1, keepdims=True) + epsilon)
    ffn_in = (rows * scale * ffng[...]).astype(BF16)
    slots = jnp.dot(chosen_ref[...], ffn_in, preferred_element_type=F32).astype(BF16)
    disp[...] = slots.reshape(disp.shape)
    sends = []
    for k in (4, 3, 5, 2, 6, 1, 7):
        e = lax.rem(z + k, 8)
        copy = remote(disp.at[e], zr.at[z // 2], dsend.at[k], drecv.at[z // 2], {"z": e})

        @pl.when(mine)
        def _(copy=copy):
            copy.start()

    for k in range(4):

        @pl.when(2 * k + c != z)
        def _(k=k):
            arrived(zr.at[k], drecv.at[k])

    @pl.when(mine)
    def _():
        zr[z // 2] = disp[z]

    packed = jnp.dot(squeeze_rows(), zr[...].reshape(32, 2 * half), preferred_element_type=F32).astype(BF16)
    home = v * 4 + u
    xg[home] = packed
    number = 0

    def share(block, device):
        nonlocal number
        copy = remote(xg.at[block], xg.at[block], gsend.at[number], grecv.at[block], device)
        copy.start()
        sends.append(copy)
        number += 1

    for k in (2, 1, 3):
        share(home, plane_id(c, lax.rem(u + k, 4), v))
    for k in (2, 1, 3):
        share(home, plane_id(c, u, lax.rem(v + k, 4)))
    for k in (1, 3, 2):
        block = v * 4 + lax.rem(u + k, 4)
        arrived(xg.at[block], grecv.at[block])
        for j in (2, 1, 3):
            share(block, plane_id(c, u, lax.rem(v + j, 4)))
    for copy in local:
        copy.wait()
    for copy in swap:
        copy.wait_recv()

    def group(step, carry):
        vv = lax.rem(v + step, 4)
        base = pl.multiple_of(vv * 4, 4)

        @pl.when(step > 0)
        def _():
            for j in range(4):
                arrived(xg.at[base + j], grecv.at[base + j])

        lhs = xg[pl.ds(base, 4)].reshape(96, 2 * half)
        pre = jnp.dot(lhs, wgu[...], preferred_element_type=F32)
        gate_pre, up_pre = pre[:, :256], pre[:, 256:]
        hidden = (gate_pre / (1.0 + jnp.exp(-gate_pre)) * up_pre).astype(BF16)
        part = jnp.dot(hidden, wd[...], preferred_element_type=F32).astype(BF16)
        po[vv] = part.reshape(4, 24, 2 * half)

        @pl.when(step > 0)
        def _():
            remote(po.at[vv], r1.at[v], psend.at[vv], precv.at[v], plane_id(c, u, vv)).start()

        return carry

    lax.fori_loop(0, 4, group, 0)
    for k in (1, 3, 2):
        vk = lax.rem(v + k, 4)
        arrived(r1.at[vk], precv.at[vk])
    for k in (2, 1, 3, 0):
        uk = lax.rem(u + k, 4)
        total = po[v, uk].astype(F32)
        for j in (1, 2, 3):
            total += r1[lax.rem(v + j, 4), uk].astype(F32)
        if k:
            ss[uk] = total.astype(BF16)
            remote(ss.at[uk], r2.at[u], ssend.at[k], srecv.at[u], plane_id(c, uk, v)).start()
    for k in (1, 3, 2):
        uk = lax.rem(u + k, 4)
        arrived(r2.at[uk], srecv.at[uk])
        total += r2[uk].astype(F32)
    ret[...] = (
        jnp.dot(spread_rows(), total.astype(BF16), preferred_element_type=F32).astype(BF16).reshape(ret.shape)
    )
    for k in range(4):
        zk = 2 * k + c
        for t in range(2):
            piece = ret.at[k, :, pl.ds(t * half, half)]
            copy = remote(piece, rb.at[z], tsend.at[k, t], trecv.at[z], {"z": zk, "tp": t})

            @pl.when(jnp.logical_or(zk != z, c != t))
            def _(copy=copy):
                copy.start()

    @pl.when(mine)
    def _():
        rb[z] = ret[z // 2, :, pl.ds(pl.multiple_of(c * half, half), half)]

    for k in (1, 7, 2, 6, 3, 5, 4):
        e = lax.rem(z + k, 8)
        arrived(rb.at[e], trecv.at[e])

    @pl.when(jnp.logical_not(mine))
    def _():
        arrived(rb.at[z], trecv.at[z])

    returned = rb[...].reshape(64, half)
    weight = weight_ref[...]
    upper = weight.astype(BF16)
    lower = (weight - upper.astype(F32)).astype(BF16)
    dims = (((0,), (0,)), ((), ()))
    mix = lax.dot_general(upper, returned, dims, preferred_element_type=F32)
    mix += lax.dot_general(lower, returned, dims, preferred_element_type=F32)
    keep = am_ref[:, pl.ds(pl.multiple_of(c * half, half), half)].astype(F32)
    out_ref[...] = (keep + mix).astype(BF16)
    for k in (4, 3, 5, 2, 6, 1, 7):

        @pl.when(mine)
        def _(k=k):
            arrived(disp.at[0], dsend.at[k])

    for copy in swap:
        copy.wait_send()
    for copy in sends:
        copy.wait_send()
    for k in (1, 2, 3):
        vk = lax.rem(v + k, 4)
        arrived(po.at[vk], psend.at[vk])
        arrived(ss.at[0], ssend.at[k])
    for k in range(4):
        for t in range(2):

            @pl.when(jnp.logical_or(2 * k + c != z, c != t))
            def _(k=k, t=t):
                arrived(rb.at[0], tsend.at[k, t])
    for copy in out + spread + back + along + ahead + home_bound:
        copy.wait_send()


def shards(
    tokens, mix_gain, query_weight, forget_weight, input_weight, lower_bound, head_gain, out_weight, state,
    ffn_gain, route_ids, route_weights, expert_gate, expert_up, expert_down,
):
    rows, width = tokens.shape
    half = width // 2
    hbm = pl.BlockSpec(memory_space=pltpu.HBM)
    vmem = pl.BlockSpec(memory_space=pltpu.VMEM)
    dma = pltpu.SemaphoreType.DMA
    scratch = lambda *shape, dtype=BF16: pltpu.VMEM(shape, dtype)
    held = lambda a: pltpu.with_memory_space_constraint(a, pltpu.HBM)
    return pl.pallas_call(
        layer_kernel,
        out_shape=(jax.ShapeDtypeStruct((rows, half), BF16), pltpu.VMEM(state.shape, F32)),
        in_specs=[hbm] * 15,
        out_specs=(vmem, vmem),
        scratch_shapes=[
            scratch(rows, width), scratch(1, width, dtype=F32), scratch(4, 128, dtype=F32), scratch(4, 128, dtype=F32),
            scratch(1, width, dtype=F32), scratch(2, 16, dtype=jnp.int32), scratch(2, 16, dtype=F32),
            scratch(4, 16, 384), scratch(8, 4, 16, 384), scratch(4, 16, 512), scratch(16, 16, 512),
            scratch(16, 16, 384), scratch(16, 16, 384), scratch(16, 128, dtype=F32),
            scratch(16, 512), scratch(8, 4, 16, 512), scratch(4, 16, 512), scratch(4, 16, 512), scratch(2, 4, 16, 512),
            scratch(rows, width), scratch(64, 16), scratch(64, 16, dtype=F32),
            scratch(width, 512), scratch(256, width), scratch(8, 8, width), scratch(4, 8, width),
            scratch(16, 24, width), scratch(4, 4, 24, width), scratch(4, 4, 24, width), scratch(4, 24, width),
            scratch(4, 24, width), scratch(4, 8, width), scratch(8, 8, half),
            dma((8,)), dma((3, 4)), dma, dma((8, 4)), dma, dma((4, 4)), dma, dma((4, 4)), dma,
            dma((8,)), dma, dma((4,)), dma, dma((4,)), dma, dma((4, 2)), dma,
            dma((3,)), dma((3,)), dma((3,)), dma((8,)), dma((4,)), dma((15,)), dma((16,)), dma((4,)), dma((4,)),
            dma((4,)), dma((4,)), dma((4, 2)), dma((8,)),
        ],
        compiler_params=pltpu.CompilerParams(
            collective_id=0, has_side_effects=True, vmem_limit_bytes=48 * 2**20
        ),
        name="layer",
    )(
        *map(held, (
            tokens, mix_gain.reshape(1, -1), query_weight, forget_weight, input_weight, lower_bound.reshape(4, 128),
            head_gain.reshape(4, 128), out_weight.T, state, ffn_gain.reshape(1, -1), route_ids.T, route_weights.T,
            expert_gate, expert_up, expert_down,
        ))
    )


def solution(mesh):
    finer = Mesh(mesh.devices.reshape(8, 4, 4, mesh.shape["tp"]), ("z", "y", "x", "tp"))
    placed = (
        P(EP, None), P(), P(EP, "tp"), P(EP, "tp"), P(EP, "tp"), P("tp"), P("tp"), P("tp", EP),
        P(EP, "tp", None, None), P(), P(EP, None), P(EP, None), P(EP, None, "tp"), P(EP, None, "tp"), P(EP, "tp", None),
    )
    return jax.shard_map(
        shards, mesh=finer, in_specs=placed, out_specs=(P(EP, "tp"), P(EP, "tp", None, None)), check_vma=False
    )
```

time: 242 us -> 93 us (0.38)
  waiting for transfers between devices: 123 us -> 0 us
  Pallas kernels: 52.1 us -> 89.7 us
  blocking collectives: 29.4 us -> 0 us
  between operations: 14.3 us -> 0.64 us
  matrix products: 12 us -> 0 us
  other arithmetic: 7.66 us -> 0 us
    all_gather x2 -> x0, waiting for transfers between devices: 123 us -> none  [the longest x1 101 us: side_by_side(): filled, at, done = (lax.all_gather(both, axis, axis=dim, tiled=True), 0, [])]
    pallas_call x1, Pallas kernels: 52.1 us -> 89.7 us  [shards(): pl.pallas_call(layer_kernel, out_shape=(jax.ShapeDtypeStruct((rows, half)...]
    all_gather x2 -> x0, blocking collectives: 21 us -> none  [gathered_by_axis(): shard = lax.all_gather(shard, axis, axis=dim, tiled=True)]
    dot_general x5 -> x0, matrix products: 12 us -> none  [the longest x3 6.16 us: shards(): jnp.dot(normed, weight_rows, preferred_element_type=jnp.float32)]
    all_to_all x1 -> x0, blocking collectives: 8.43 us -> none  [sent_to_all(): return lax.all_to_all(copies, axis, split_axis=0, concat_axis=0, tiled=True)]
    add x1 -> x0, other arithmetic: 4.39 us -> none  [shards(): forget[..., None] * state]
  transfers between devices with their start and end apart: 2 -> 0, of which waited for: 2 -> 0; matrix products, arithmetic and copies ran while one was open for 7% -> 0% of each run, Pallas kernels for 0% -> 0%
where the time goes in v2:
time: 93 us; the launch traced here: 92.9 us
  Pallas kernels  89.7 us (96%)
  local copies, waits for them, and re-layouts  2.63 us (3%)
    pallas_call x1, Pallas kernels, shards(): pl.pallas_call(layer_kernel, out_shape=(jax.ShapeDtypeStruct((rows, half)...  89.7 us
    unnamed x2, local copies, waits for them, and re-layouts  2.63 us

profile of v2, /device:TPU:1, one launch (start us, length us, event | category | flops | bytes accessed | tf_op | source)
XLA Modules:
  0.0 92.9 jit_solution(6415354026764894105)
XLA Ops:
  0.6 89.7 %layer.1 = (bf16[16,1024]{1,0:T(8,128)(2,1)S(1)}, f32[16,4,128,128]{3,2,1,0:T(8,128)S(1)}) custom-call(bf16[16,2048]{1,0:T(8,128)(2,1)} %tok_hbm.1, f32[1,2048]{1,0:T(1,128)} %bitcast.8, bf16[16,512]{1,0:T(8,128)(2,1)} %qw_hbm.1, bf16[16,512]{1,0:T(8,128)(2,1)} %fw_hbm.1, bf16[16,512]{1,0:T(8,128)(2,1)} %iw_hbm.1, f32[4,128]{1,0:T(4,128)} %bitcast.10, ...), custom_call_target="tpu_custom_call" | custom-call | tf_op jit(solution)/shard_map/layer/pallas_call | solution.py:411
  90.3 2.0 %copy.19 = f32[16,4,128,128]{3,2,1,0:T(8,128)} copy(f32[16,4,128,128]{3,2,1,0:T(8,128)S(1)} %get-tuple-element.3) | data formatting | bytes 8388608
  92.3 0.6 copy.20

commit v3 on v2

v3 whole, which is shorter than its diff:
```python
import functools
import jax
import jax.numpy as jnp
from jax import lax
from jax.experimental import pallas as pl
from jax.experimental.pallas import tpu as pltpu
from jax.sharding import Mesh
from jax.sharding import PartitionSpec as P

EXPERTS = 8
TOP = 2
EP = ("z", "y", "x")
MESH_ID = pl.DeviceIdType.MESH
F32 = jnp.float32
BF16 = jnp.bfloat16
epsilon = 1e-06
FILLED = 6


def place():
    c, z = lax.axis_index("tp"), lax.axis_index("z")
    y, x = lax.axis_index("y"), lax.axis_index("x")
    first = c == 0
    return c, z, y, x, jnp.where(first, x, y), jnp.where(first, y, x)


def plane_id(c, u, v):
    first = c == 0
    return {"x": jnp.where(first, u, v), "y": jnp.where(first, v, u)}


def remote(src, dst, send, recv, device):
    return pltpu.make_async_remote_copy(
        src_ref=src, dst_ref=dst, send_sem=send, recv_sem=recv, device_id=device, device_id_type=MESH_ID
    )


def arrived(ref, sem):
    pltpu.make_async_copy(ref, ref, sem).wait()


def route_slots(ids_ref, wts_ref):
    row = lax.broadcasted_iota(jnp.int32, (64, 16), 0)
    expert, slot = row // 8, row % 8
    pick0 = (jnp.broadcast_to(ids_ref[0:1, :], (64, 16)) == expert).astype(F32)
    pick1 = (jnp.broadcast_to(ids_ref[1:2, :], (64, 16)) == expert).astype(F32)
    pick = pick0 + pick1
    earlier = (
        lax.broadcasted_iota(jnp.int32, (16, 16), 0) < lax.broadcasted_iota(jnp.int32, (16, 16), 1)
    ).astype(F32)
    rank = jnp.dot(pick, earlier, preferred_element_type=F32)
    chosen = jnp.where(rank == slot.astype(F32), pick, 0.0)
    weight = pick0 * jnp.broadcast_to(wts_ref[0:1, :], (64, 16)) + pick1 * jnp.broadcast_to(wts_ref[1:2, :], (64, 16))
    return chosen, chosen * weight


def squeeze_rows():
    to = lax.broadcasted_iota(jnp.int32, (24, 32), 0)
    frm = lax.broadcasted_iota(jnp.int32, (24, 32), 1)
    return (((to // 6) * 8 + to % 6) == frm).astype(BF16)


def spread_rows():
    to = lax.broadcasted_iota(jnp.int32, (32, 24), 0)
    frm = lax.broadcasted_iota(jnp.int32, (32, 24), 1)
    return (((frm // 6) * 8 + frm % 6) == to).astype(BF16)


def halves(left, right, odd):
    lane = lax.broadcasted_iota(jnp.int32, left.shape, 1)
    if odd:
        left = pltpu.roll(left, 64, 1)
    else:
        right = pltpu.roll(right, 64, 1)
    return jnp.where(lane < 64, left, right)


class Ledger:
    def __init__(self):
        self.open = {}
        self.seen = set()

    def expect(self, key, wait):
        self.open[key] = wait
        self.seen.add(key)

    def wait(self, *keys):
        for key in keys:
            self.open.pop(key)()

    def finish(self):
        for wait in self.open.values():
            wait()
        self.open = {}


def only(condition, do):
    return lambda: pl.when(condition)(do)


def either(condition, these, others, sem):
    def wait():
        pl.when(condition)(lambda: arrived(these, sem))
        pl.when(jnp.logical_not(condition))(lambda: arrived(others, sem))

    return wait


def layer_kernel(
    tok_hbm, mixg_hbm, qw_hbm, fw_hbm, iw_hbm, lb_hbm, hg_hbm, wo_hbm, st_hbm, ffng_hbm, ids_hbm, wts_hbm,
    gate_ref, up_ref, down_ref, out_ref, st,
    tok, mixg, lb, hg, ffng, ids_ref, wts_ref, wcat, wb, xs, xb, ob, qb, ro, ho, wob, hb, pb, mb, am_ref, chosen_ref, weight_ref,
    wgu, wd, disp, zr, xg, po, pr, ss, r2, ret, rb,
    lsem, qsem, stsem, wsend, wrecv, xsend, xrecv, osend, orecv, wozs, wozr, woxs, woxr, hsend, hrecv, msend, mrecv,
    lwsem, swsend, swrecv, dsend, drecv, gsend, gu, gv, psend, precv, ssend, srecv, tsend, trecv,
):
    c, z, y, x, u, v = place()
    half = out_ref.shape[1]
    mine = lax.rem(z, 2) == c
    other = 1 - c
    spot = y * 4 + x
    bar = pltpu.get_barrier_semaphore()
    peers = [{"tp": other}]
    for dz in range(8):
        zk = lax.rem(z + dz, 8)
        for dx in range(4):
            if dz or dx:
                peers.append({"z": zk, "x": lax.rem(x + dx, 4)})
        if dz:
            peers.append({"z": zk, "tp": other})
    for dy in range(1, 4):
        yk = lax.rem(y + dy, 4)
        for dx in range(4):
            peers.append({"y": yk, "x": lax.rem(x + dx, 4)})
        peers.append({"y": yk, "tp": other})
    for device in peers:
        pl.semaphore_signal(bar, inc=1, device_id=device, device_id_type=MESH_ID)
    loads = [
        pltpu.make_async_copy(a, b, lsem.at[i])
        for i, (a, b) in enumerate(
            ((tok_hbm, tok), (mixg_hbm, mixg), (lb_hbm, lb), (hg_hbm, hg), (ffng_hbm, ffng), (ids_hbm, ids_ref), (wts_hbm, wts_ref),
             (wo_hbm, wob.at[z, x]))
        )
    ]
    own = pl.ds(pl.multiple_of(c * 128, 128), 128)
    own_up = pl.ds(pl.multiple_of(256 + c * 128, 128), 128)
    pieces = []
    for i, w_hbm in enumerate((qw_hbm, fw_hbm, iw_hbm)):
        for h in range(4):
            pieces.append(
                pltpu.make_async_copy(w_hbm.at[:, pl.ds(h * 128, 128)], wcat.at[h, :, pl.ds(i * 128, 128)], qsem)
            )
    led = Ledger()
    for i, copy in enumerate(loads[:2] + pieces + loads[2:]):
        copy.start()
    for i, copy in enumerate(loads):
        led.expect(("load", i), copy.wait)
    led.expect("pieces", lambda: arrived(wcat, qsem))
    local = [
        pltpu.make_async_copy(gate_ref.at[0], wgu.at[:, own], lwsem),
        pltpu.make_async_copy(up_ref.at[0], wgu.at[:, own_up], lwsem),
        pltpu.make_async_copy(down_ref.at[0], wd.at[own, :], lwsem),
    ]
    state_in = pltpu.make_async_copy(st_hbm, st, stsem)
    state_in.start()
    led.expect("state", state_in.wait)
    for copy in local:
        copy.start()
    led.expect("local", lambda: arrived(wgu.at[:, pl.ds(0, 384)], lwsem))
    led.wait(("load", 0), ("load", 1))
    tokens = tok[...].astype(F32)
    scale = lax.rsqrt(jnp.mean(tokens * tokens, axis=-1, keepdims=True) + epsilon)
    normed = tokens * scale * mixg[...]
    for yk in range(4):
        for j in range(4):
            a, b = 4 * j + yk // 2, 4 * j + 2 + yk // 2
            xs[yk, :, pl.ds(j * 128, 128)] = halves(
                normed[:, a * 128 : a * 128 + 128], normed[:, b * 128 : b * 128 + 128], yk % 2
            ).astype(BF16)
    led.wait("pieces")
    zr[...] = jnp.zeros_like(zr)
    rb[...] = jnp.zeros_like(rb)
    pl.semaphore_wait(bar, len(peers))
    out = []
    for dz in (4, 3, 5, 2, 6, 1, 7, 0):
        for dx in (2, 1, 3, 0):
            if dz or dx:
                xk = lax.rem(x + dx, 4)
                out.append(remote(wcat.at[xk], wb.at[z, x], wsend, wrecv, {"z": lax.rem(z + dz, 8), "x": xk}))
    for dy in (2, 1, 3, 0):
        for dx in (2, 1, 3, 0):
            if dy or dx:
                yk = lax.rem(y + dy, 4)
                out.append(remote(xs.at[yk], xb.at[spot], xsend, xrecv, {"y": yk, "x": lax.rem(x + dx, 4)}))
    for copy in out:
        copy.start()
    wbf = wb.reshape(32, 16, 384)
    led.expect("x out", lambda: arrived(xb.at[pl.ds(0, 15)], xsend))
    led.expect("w out", lambda: arrived(wbf.at[pl.ds(0, 31)], wsend))
    led.expect("x", lambda: arrived(xb.at[pl.ds(0, 15)], xrecv))
    led.expect("w", lambda: arrived(wbf.at[pl.ds(0, 31)], wrecv))
    wb[z, x] = wcat[x]
    xb[spot] = xs[y]
    led.wait(*(("load", i) for i in range(2, 8)))
    spread = []
    for k in (4, 3, 5, 2, 6, 1, 7):
        spread.append(remote(wob.at[z, x], wob.at[z, x], wozs, wozr, {"z": lax.rem(z + k, 8)}))
    for copy in spread:
        copy.start()
    led.expect("woz out", lambda: arrived(xb.at[pl.ds(0, 7)], wozs))
    led.expect("woz", lambda: arrived(xb.at[pl.ds(0, 7)], wozr))
    swap = [
        remote(gate_ref.at[0], wgu.at[:, own], swsend, swrecv, {"tp": other}),
        remote(up_ref.at[0], wgu.at[:, own_up], swsend, swrecv, {"tp": other}),
        remote(down_ref.at[0], wd.at[own, :], swsend, swrecv, {"tp": other}),
    ]
    for copy in swap:
        copy.start()
    led.expect("swap out", lambda: arrived(wgu.at[:, pl.ds(0, 384)], swsend))
    led.expect("swap in", lambda: arrived(wgu.at[:, pl.ds(0, 384)], swrecv))
    chosen, weight = route_slots(ids_ref, wts_ref)
    chosen_ref[...] = chosen.astype(BF16)
    weight_ref[...] = weight
    led.wait("x", "w")
    part = jnp.dot(xb[...].reshape(256, 512), wbf[...].reshape(512, 384), preferred_element_type=F32)
    ob[...] = part.astype(BF16).reshape(16, 16, 384)
    back = []
    for dy in (2, 1, 3, 0):
        for dx in (2, 1, 3, 0):
            if dy or dx:
                yk, xk = lax.rem(y + dy, 4), lax.rem(x + dx, 4)
                back.append(remote(ob.at[yk * 4 + xk], qb.at[spot], osend, orecv, {"y": yk, "x": xk}))
    for copy in back:
        copy.start()
    led.expect("q out", lambda: arrived(qb.at[pl.ds(0, 15)], osend))
    led.expect("q", lambda: arrived(qb.at[pl.ds(0, 15)], orecv))
    qb[spot] = ob[spot]
    led.wait("woz")
    along = []
    for k in (2, 1, 3):
        along.append(remote(wob.at[:, x], wob.at[:, x], woxs, woxr, {"x": lax.rem(x + k, 4)}))
    for copy in along:
        copy.start()
    led.expect("wox out", lambda: arrived(wob.at[:, pl.ds(0, 3)], woxs))
    led.expect("wox", lambda: arrived(wob.at[:, pl.ds(0, 3)], woxr))
    led.wait("state", "q")

    def head(h, carry):
        qfv = (
            qb[h].astype(F32) + qb[4 + h].astype(F32) + qb[8 + h].astype(F32) + qb[12 + h].astype(F32)
        )
        bound = lb[pl.ds(h, 1), :]
        forget = bound + (1.0 - bound) * (1.0 / (1.0 + jnp.exp(-qfv[:, 128:256])))
        fresh = qfv[:, 256:384]
        q_t = qfv[:, 0:128].T
        f_t = forget.T
        for s in range(16):
            f_col = jnp.broadcast_to(f_t[:, s : s + 1], (128, 128))
            q_col = jnp.broadcast_to(q_t[:, s : s + 1], (128, 128))
            row = fresh[s : s + 1, :]
            new = row + f_col * (st[s, h] - row)
            st[s, h] = new
            ro[s : s + 1, :] = jnp.sum(q_col * new, axis=0, keepdims=True)
        read = ro[...]
        read = read * lax.rsqrt(jnp.mean(read * read, axis=-1, keepdims=True) + epsilon) * hg[pl.ds(h, 1), :]
        ho[:, pl.ds(pl.multiple_of(h * 128, 128), 128)] = read.astype(BF16)
        return carry

    lax.fori_loop(0, 4, head, 0)
    ahead = []
    for k in (2, 1, 3):
        ahead.append(remote(ho, hb.at[y], hsend, hrecv, {"y": lax.rem(y + k, 4)}))
    for copy in ahead:
        copy.start()
    led.expect("h out", lambda: arrived(hb.at[pl.ds(0, 3)], hsend))
    led.expect("h", lambda: arrived(hb.at[pl.ds(0, 3)], hrecv))
    hb[y] = ho[...]
    led.wait("wox", "h")
    dims = (((1,), (1,)), ((), ()))
    mixed = lax.dot_general(
        hb[...].reshape(64, 512), wob[...].reshape(512, 512), dims, preferred_element_type=F32
    )
    pb[...] = mixed.astype(BF16).reshape(4, 16, 512)
    home_bound = []
    for k in (2, 1, 3, 0):
        yk = lax.rem(y + k, 4)
        for t in (0, 1):
            if k or t:
                device = {"y": yk, "tp": lax.rem(c + t, 2)}
                home_bound.append(remote(pb.at[yk], mb.at[c, y], msend, mrecv, device))
    for copy in home_bound:
        copy.start()
    led.expect("m out", lambda: arrived(mb.reshape(8, 16, 512).at[pl.ds(0, 7)], msend))
    led.expect("m", lambda: arrived(mb.reshape(8, 16, 512).at[pl.ds(0, 7)], mrecv))
    mb[c, y] = pb[y]
    led.wait("m")
    sums = [mb[0, k].astype(F32) + mb[1, k].astype(F32) for k in range(4)]
    for zk in range(8):
        at = (zk // 2) * 128
        for h in range(2):
            cols = pl.ds(zk * 256 + h * 128, 128)
            got = halves(sums[2 * h][:, at : at + 128], sums[2 * h + 1][:, at : at + 128], zk % 2)
            am_ref[:, cols] = (tok[:, cols].astype(F32) + got).astype(BF16)
    rows = am_ref[...].astype(F32)
    scale = lax.rsqrt(jnp.mean(rows * rows, axis=-1, keepdims=True) + epsilon)
    ffn_in = (rows * scale * ffng[...]).astype(BF16)
    slots = jnp.dot(chosen_ref[...], ffn_in, preferred_element_type=F32).astype(BF16)
    disp[...] = slots.reshape(disp.shape)
    halves_at = [pl.ds(w * half, half) for w in range(2)]
    for w in range(2):
        for k in (4, 3, 5, 2, 6, 1, 7):
            e = lax.rem(z + k, 8)
            piece = disp.at[e, pl.ds(0, FILLED), halves_at[w]]
            copy = remote(piece, zr.at[w, z // 2, pl.ds(0, FILLED)], dsend, drecv.at[w], {"z": e})

            @pl.when(mine)
            def _(copy=copy):
                copy.start()

        led.expect(("slots", w), either(mine, zr.at[w, pl.ds(0, 3), pl.ds(0, FILLED)], zr.at[w, :, pl.ds(0, FILLED)], drecv.at[w]))
    led.expect("slots out", only(mine, lambda: arrived(disp.at[pl.ds(0, 7), pl.ds(0, FILLED)], dsend)))

    @pl.when(mine)
    def _():
        for w in range(2):
            zr[w, z // 2] = disp[z, :, halves_at[w]]

    lines = [lax.rem(u + j, 4) for j in range(4)]
    across = [lax.rem(v + k, 4) for k in range(4)]
    for w in range(2):
        for j in range(4):
            uj = lines[j]
            if j:
                led.expect(("rows", w, j, 0), lambda w=w, uj=uj: arrived(xg.at[w * 16 + uj * 4 + v], gu.at[w, uj]))
            led.expect(("rows", w, j, 1), lambda w=w, uj=uj: arrived(xg.at[pl.ds(0, 3)], gv.at[w, uj]))
    led.expect("rows out", lambda: arrived(xg.at[pl.ds(0, 30)], gsend))
    led.expect("parts out", lambda: arrived(xg.at[pl.ds(0, 24)], psend))
    led.expect("sums out", lambda: arrived(xg.at[pl.ds(0, 6)], ssend))

    def along_v(w, j):
        block = xg.at[w * 16 + lines[j] * 4 + v]
        for k in (2, 1, 3):
            remote(block, block, gsend, gv.at[w, lines[j]], plane_id(c, u, across[k])).start()

    def from_z(w):
        led.wait(("slots", w))
        packed = jnp.dot(squeeze_rows(), zr[w].reshape(32, half), preferred_element_type=F32).astype(BF16)
        xg[w * 16 + u * 4 + v] = packed
        block = xg.at[w * 16 + u * 4 + v]
        for k in (2, 1, 3):
            remote(block, block, gsend, gu.at[w, u], plane_id(c, lines[k], v)).start()
        along_v(w, 0)

    def from_u(w, j):
        led.wait(("rows", w, j, 0))
        along_v(w, j)

    def first(w, j):
        led.wait(("rows", w, j, 1))
        rows_in = xg[pl.ds(w * 16 + lines[j] * 4, 4)].reshape(96, half)
        return jnp.dot(rows_in, wgu[halves_at[w], :], preferred_element_type=F32)

    def second(j):
        uj = lines[j]
        pre = first(0, j) + first(1, j)
        gate_pre, up_pre = pre[:, :256], pre[:, 256:]
        hidden = (gate_pre / (1.0 + jnp.exp(-gate_pre)) * up_pre).astype(BF16)
        for w in range(2):
            part = jnp.dot(hidden, wd[:, halves_at[w]], preferred_element_type=F32).astype(BF16)
            po[w, uj] = part.reshape(4, 24, half)
            for k in (2, 1, 3):
                there = plane_id(c, u, across[k])
                remote(po.at[w, uj, across[k]], pr.at[w, uj, v], psend, precv.at[w, uj], there).start()
            led.expect(("part in", w, j), lambda w=w: arrived(pr.at[w, uj, pl.ds(0, 3)], precv.at[w, uj]))

    def gather(w, j):
        uj = lines[j]
        led.wait(("part in", w, j))
        total = po[w, uj, v].astype(F32)
        for k in (1, 3, 2):
            total += pr[w, uj, across[k]].astype(F32)
        return total

    def hand_over(w, j):
        uj = lines[j]
        ss[w, uj] = gather(w, j).astype(BF16)
        remote(ss.at[w, uj], r2.at[w, u], ssend, srecv.at[w], plane_id(c, uj, v)).start()

    def give_back(w):
        total = gather(w, 0)
        arrived(r2.at[w, pl.ds(0, 3)], srecv.at[w])
        for k in (1, 3, 2):
            total += r2[w, lines[k]].astype(F32)
        ret[:, :, halves_at[w]] = (
            jnp.dot(spread_rows(), total.astype(BF16), preferred_element_type=F32).astype(BF16).reshape(4, 8, half)
        )
        for k in (2, 1, 3, 0):
            at = lax.rem(z // 2 + k, 4)
            zk = 2 * at + c
            piece = ret.at[at, pl.ds(0, FILLED), halves_at[w]]
            copy = remote(piece, rb.at[z, pl.ds(0, FILLED)], tsend, trecv, {"z": zk, "tp": w})
            away = jnp.logical_or(zk != z, c != w)

            @pl.when(away)
            def _(copy=copy):
                copy.start()


    from_z(0)
    from_z(1)
    led.wait("local", "swap in")
    from_u(0, 3)
    from_u(0, 1)
    from_u(0, 2)
    from_u(1, 3)
    from_u(1, 1)
    from_u(1, 2)
    second(0)
    second(3)
    second(1)
    second(2)
    for j in (3, 1, 2):
        for w in range(2):
            hand_over(w, j)
    give_back(0)
    give_back(1)

    @pl.when(mine)
    def _():
        rb[z] = ret[z // 2, :, pl.ds(pl.multiple_of(c * half, half), half)]

    seven, eight = rb.at[pl.ds(0, 7), pl.ds(0, FILLED)], rb.at[:, pl.ds(0, FILLED)]
    either(mine, seven, eight, trecv)()
    led.expect("returned out", either(mine, seven, eight, tsend))
    returned = rb[...].reshape(64, half)
    weight = weight_ref[...]
    upper = weight.astype(BF16)
    lower = (weight - upper.astype(F32)).astype(BF16)
    dims = (((0,), (0,)), ((), ()))
    mix = lax.dot_general(upper, returned, dims, preferred_element_type=F32)
    mix += lax.dot_general(lower, returned, dims, preferred_element_type=F32)
    keep = am_ref[:, pl.ds(pl.multiple_of(c * half, half), half)].astype(F32)
    out_ref[...] = (keep + mix).astype(BF16)
    led.finish()


def shards(
    tokens, mix_gain, query_weight, forget_weight, input_weight, lower_bound, head_gain, out_weight, state,
    ffn_gain, route_ids, route_weights, expert_gate, expert_up, expert_down,
):
    rows, width = tokens.shape
    half = width // 2
    hbm = pl.BlockSpec(memory_space=pltpu.HBM)
    vmem = pl.BlockSpec(memory_space=pltpu.VMEM)
    dma = pltpu.SemaphoreType.DMA
    scratch = lambda *shape, dtype=BF16: pltpu.VMEM(shape, dtype)
    held = lambda a: pltpu.with_memory_space_constraint(a, pltpu.HBM)
    return pl.pallas_call(
        layer_kernel,
        out_shape=(jax.ShapeDtypeStruct((rows, half), BF16), pltpu.VMEM(state.shape, F32)),
        in_specs=[hbm] * 15,
        out_specs=(vmem, vmem),
        scratch_shapes=[
            scratch(rows, width), scratch(1, width, dtype=F32), scratch(4, 128, dtype=F32), scratch(4, 128, dtype=F32),
            scratch(1, width, dtype=F32), scratch(2, 16, dtype=jnp.int32), scratch(2, 16, dtype=F32),
            scratch(4, 16, 384), scratch(8, 4, 16, 384), scratch(4, 16, 512), scratch(16, 16, 512),
            scratch(16, 16, 384), scratch(16, 16, 384), scratch(16, 128, dtype=F32),
            scratch(16, 512), scratch(8, 4, 16, 512), scratch(4, 16, 512), scratch(4, 16, 512), scratch(2, 4, 16, 512),
            scratch(rows, width), scratch(64, 16), scratch(64, 16, dtype=F32),
            scratch(width, 512), scratch(256, width), scratch(8, 8, width), scratch(2, 4, 8, half),
            scratch(32, 24, half), scratch(2, 4, 4, 24, half), scratch(2, 4, 4, 24, half), scratch(2, 4, 24, half),
            scratch(2, 4, 24, half),
            scratch(4, 8, width), scratch(8, 8, half),
            dma((8,)), *[dma] * 16,
            *[dma] * 3, dma, dma((2,)), dma, dma((2, 4)), dma((2, 4)), dma, dma((2, 4)), dma, dma((2,)), dma, dma,
        ],
        compiler_params=pltpu.CompilerParams(
            collective_id=0, has_side_effects=True, vmem_limit_bytes=48 * 2**20
        ),
        name="layer",
    )(
        *map(held, (
            tokens, mix_gain.reshape(1, -1), query_weight, forget_weight, input_weight, lower_bound.reshape(4, 128),
            head_gain.reshape(4, 128), out_weight.T, state, ffn_gain.reshape(1, -1), route_ids.T, route_weights.T,
            expert_gate, expert_up, expert_down,
        ))
    )


def solution(mesh):
    finer = Mesh(mesh.devices.reshape(8, 4, 4, mesh.shape["tp"]), ("z", "y", "x", "tp"))
    placed = (
        P(EP, None), P(), P(EP, "tp"), P(EP, "tp"), P(EP, "tp"), P("tp"), P("tp"), P("tp", EP),
        P(EP, "tp", None, None), P(), P(EP, None), P(EP, None), P(EP, None, "tp"), P(EP, None, "tp"), P(EP, "tp", None),
    )
    return jax.shard_map(
        shards, mesh=finer, in_specs=placed, out_specs=(P(EP, "tp"), P(EP, "tp", None, None)), check_vma=False
    )
```

time: 93 us -> 82.9 us (0.89)
  Pallas kernels: 89.7 us -> 79.5 us
    pallas_call x1, Pallas kernels: 89.7 us -> 79.5 us  [shards(): pl.pallas_call(layer_kernel, out_shape=(jax.ShapeDtypeStruct((rows, half)...]
where the time goes in v3:
time: 82.9 us; the launch traced here: 82.8 us
  Pallas kernels  79.5 us (96%)
  local copies, waits for them, and re-layouts  2.63 us (3%)
    pallas_call x1, Pallas kernels, shards(): pl.pallas_call(layer_kernel, out_shape=(jax.ShapeDtypeStruct((rows, half)...  79.5 us
    unnamed x2, local copies, waits for them, and re-layouts  2.63 us

profile of v3, /device:TPU:1, one launch (start us, length us, event | category | flops | bytes accessed | tf_op | source)
XLA Modules:
  0.0 82.8 jit_solution(13093602448791677629)
XLA Ops:
  0.6 79.5 %layer.1 = (bf16[16,1024]{1,0:T(8,128)(2,1)S(1)}, f32[16,4,128,128]{3,2,1,0:T(8,128)S(1)}) custom-call(bf16[16,2048]{1,0:T(8,128)(2,1)} %tok_hbm.1, f32[1,2048]{1,0:T(1,128)} %bitcast.8, bf16[16,512]{1,0:T(8,128)(2,1)} %qw_hbm.1, bf16[16,512]{1,0:T(8,128)(2,1)} %fw_hbm.1, bf16[16,512]{1,0:T(8,128)(2,1)} %iw_hbm.1, f32[4,128]{1,0:T(4,128)} %bitcast.10, ...), custom_call_target="tpu_custom_call" | custom-call | tf_op jit(solution)/shard_map/layer/pallas_call | solution.py:458
  80.1 2.0 %copy.19 = f32[16,4,128,128]{3,2,1,0:T(8,128)} copy(f32[16,4,128,128]{3,2,1,0:T(8,128)S(1)} %get-tuple-element.3) | data formatting | bytes 8388608
  82.2 0.6 copy.20

commit v4 on v3

--- a/solution.py
+++ b/solution.py
@@ -109,7 +109,7 @@
 def layer_kernel(
     tok_hbm, mixg_hbm, qw_hbm, fw_hbm, iw_hbm, lb_hbm, hg_hbm, wo_hbm, st_hbm, ffng_hbm, ids_hbm, wts_hbm,
     gate_ref, up_ref, down_ref, out_ref, st,
-    tok, mixg, lb, hg, ffng, ids_ref, wts_ref, wcat, wb, xs, xb, ob, qb, ro, ho, wob, hb, pb, mb, am_ref, chosen_ref, weight_ref,
+    tok, mixg, lb, hg, ffng, ids_ref, wts_ref, wcat, wb, xs, xb, ob, qb, fan, fresh, terms, ro, ho, wob, hb, pb, mb, am_ref, chosen_ref, weight_ref,
     wgu, wd, disp, zr, xg, po, pr, ss, r2, ret, rb,
     lsem, qsem, stsem, wsend, wrecv, xsend, xrecv, osend, orecv, wozs, wozr, woxs, woxr, hsend, hrecv, msend, mrecv,
     lwsem, swsend, swrecv, dsend, drecv, gsend, gu, gv, psend, precv, ssend, srecv, tsend, trecv,
@@ -119,6 +119,8 @@
     mine = lax.rem(z, 2) == c
     other = 1 - c
     spot = y * 4 + x
+    side, row_of = lax.rem(z, 2), z // 2
+    pair = [lax.rem(side + i, 2) + 2 * row_of for i in range(2)]
     bar = pltpu.get_barrier_semaphore()
     peers = [{"tp": other}]
     for dz in range(8):
@@ -133,13 +135,15 @@
         for dx in range(4):
             peers.append({"y": yk, "x": lax.rem(x + dx, 4)})
         peers.append({"y": yk, "tp": other})
+        peers.append({"y": yk, "z": pair[1]})
+        peers.append({"y": yk, "z": pair[1], "tp": other})
     for device in peers:
         pl.semaphore_signal(bar, inc=1, device_id=device, device_id_type=MESH_ID)
     loads = [
         pltpu.make_async_copy(a, b, lsem.at[i])
         for i, (a, b) in enumerate(
             ((tok_hbm, tok), (mixg_hbm, mixg), (lb_hbm, lb), (hg_hbm, hg), (ffng_hbm, ffng), (ids_hbm, ids_ref), (wts_hbm, wts_ref),
-             (wo_hbm, wob.at[z, x]))
+             (wo_hbm, wob.at[row_of, x]))
         )
     ]
     own = pl.ds(pl.multiple_of(c * 128, 128), 128)
@@ -178,6 +182,8 @@
                 normed[:, a * 128 : a * 128 + 128], normed[:, b * 128 : b * 128 + 128], yk % 2
             ).astype(BF16)
     led.wait("pieces")
+    ones_at = lax.broadcasted_iota(jnp.int32, fan.shape, 0) % 16 == lax.broadcasted_iota(jnp.int32, fan.shape, 1) // 128
+    fan[...] = ones_at.astype(BF16)
     zr[...] = jnp.zeros_like(zr)
     rb[...] = jnp.zeros_like(rb)
     pl.semaphore_wait(bar, len(peers))
@@ -203,12 +209,13 @@
     xb[spot] = xs[y]
     led.wait(*(("load", i) for i in range(2, 8)))
     spread = []
-    for k in (4, 3, 5, 2, 6, 1, 7):
-        spread.append(remote(wob.at[z, x], wob.at[z, x], wozs, wozr, {"z": lax.rem(z + k, 8)}))
+    for k in (4, 2, 6):
+        block = wob.at[row_of, x]
+        spread.append(remote(block, block, wozs, wozr, {"z": lax.rem(z + k, 8)}))
     for copy in spread:
         copy.start()
-    led.expect("woz out", lambda: arrived(xb.at[pl.ds(0, 7)], wozs))
-    led.expect("woz", lambda: arrived(xb.at[pl.ds(0, 7)], wozr))
+    led.expect("woz out", lambda: arrived(xb.at[pl.ds(0, 3)], wozs))
+    led.expect("woz", lambda: arrived(xb.at[pl.ds(0, 3)], wozr))
     swap = [
         remote(gate_ref.at[0], wgu.at[:, own], swsend, swrecv, {"tp": other}),
         remote(up_ref.at[0], wgu.at[:, own_up], swsend, swrecv, {"tp": other}),
@@ -245,62 +252,68 @@
     led.expect("wox", lambda: arrived(wob.at[:, pl.ds(0, 3)], woxr))
     led.wait("state", "q")
 
-    def head(h, carry):
-        qfv = (
-            qb[h].astype(F32) + qb[4 + h].astype(F32) + qb[8 + h].astype(F32) + qb[12 + h].astype(F32)
-        )
-        bound = lb[pl.ds(h, 1), :]
+    for h in range(4):
+        qfv = qb[h].astype(F32) + qb[4 + h].astype(F32) + qb[8 + h].astype(F32) + qb[12 + h].astype(F32)
+        bound = lb[h : h + 1, :]
         forget = bound + (1.0 - bound) * (1.0 / (1.0 + jnp.exp(-qfv[:, 128:256])))
-        fresh = qfv[:, 256:384]
-        q_t = qfv[:, 0:128].T
-        f_t = forget.T
-        for s in range(16):
-            f_col = jnp.broadcast_to(f_t[:, s : s + 1], (128, 128))
-            q_col = jnp.broadcast_to(q_t[:, s : s + 1], (128, 128))
-            row = fresh[s : s + 1, :]
-            new = row + f_col * (st[s, h] - row)
-            st[s, h] = new
-            ro[s : s + 1, :] = jnp.sum(q_col * new, axis=0, keepdims=True)
-        read = ro[...]
-        read = read * lax.rsqrt(jnp.mean(read * read, axis=-1, keepdims=True) + epsilon) * hg[pl.ds(h, 1), :]
-        ho[:, pl.ds(pl.multiple_of(h * 128, 128), 128)] = read.astype(BF16)
-        return carry
-
-    lax.fori_loop(0, 4, head, 0)
+        fresh[h] = qfv[:, 256:384]
+        for i, value in enumerate((qfv[:, 0:128], forget)):
+            upper = value.astype(BF16).astype(F32)
+            terms[i, h] = jnp.concatenate([upper, value - upper], axis=0).T.astype(BF16)
+    for h in range(4):
+        for p in range(8):
+            across_lanes = fan[:, 256 * p : 256 * p + 256]
+            q_cols = jnp.dot(terms[0, h], across_lanes, preferred_element_type=F32)
+            f_cols = jnp.dot(terms[1, h], across_lanes, preferred_element_type=F32)
+            for i in range(2):
+                s, lanes = 2 * p + i, slice(128 * i, 128 * i + 128)
+                row = fresh[h, s : s + 1, :]
+                new = row + f_cols[:, lanes] * (st[s, h] - row)
+                st[s, h] = new
+                ro[h, s : s + 1, :] = jnp.sum(q_cols[:, lanes] * new, axis=0, keepdims=True)
+    for h in range(4):
+        read = ro[h]
+        read = read * lax.rsqrt(jnp.mean(read * read, axis=-1, keepdims=True) + epsilon) * hg[h : h + 1, :]
+        ho[:, h * 128 : h * 128 + 128] = read.astype(BF16)
+    group = [(k, i) for k in (2, 1, 3, 0) for i in (1, 0)]
     ahead = []
-    for k in (2, 1, 3):
-        ahead.append(remote(ho, hb.at[y], hsend, hrecv, {"y": lax.rem(y + k, 4)}))
+    for k, i in group[:-1]:
+        ahead.append(remote(ho, hb.at[side, y], hsend, hrecv, {"y": lax.rem(y + k, 4), "z": pair[i]}))
     for copy in ahead:
         copy.start()
-    led.expect("h out", lambda: arrived(hb.at[pl.ds(0, 3)], hsend))
-    led.expect("h", lambda: arrived(hb.at[pl.ds(0, 3)], hrecv))
-    hb[y] = ho[...]
+    hbf = hb.reshape(8, 16, 512)
+    led.expect("h out", lambda: arrived(hbf.at[pl.ds(0, 7)], hsend))
+    led.expect("h", lambda: arrived(hbf.at[pl.ds(0, 7)], hrecv))
+    hb[side, y] = ho[...]
     led.wait("wox", "h")
     dims = (((1,), (1,)), ((), ()))
     mixed = lax.dot_general(
-        hb[...].reshape(64, 512), wob[...].reshape(512, 512), dims, preferred_element_type=F32
+        hb[...].reshape(128, 512), wob[...].reshape(256, 512), dims, preferred_element_type=F32
     )
-    pb[...] = mixed.astype(BF16).reshape(4, 16, 512)
+    pb[...] = mixed.astype(BF16).reshape(2, 4, 16, 256)
     home_bound = []
-    for k in (2, 1, 3, 0):
+    for k, i in group:
         yk = lax.rem(y + k, 4)
         for t in (0, 1):
-            if k or t:
-                device = {"y": yk, "tp": lax.rem(c + t, 2)}
-                home_bound.append(remote(pb.at[yk], mb.at[c, y], msend, mrecv, device))
+            if k or i or t:
+                device = {"y": yk, "z": pair[i], "tp": lax.rem(c + t, 2)}
+                home_bound.append(remote(pb.at[lax.rem(side + i, 2), yk], mb.at[c, side, y], msend, mrecv, device))
     for copy in home_bound:
         copy.start()
-    led.expect("m out", lambda: arrived(mb.reshape(8, 16, 512).at[pl.ds(0, 7)], msend))
-    led.expect("m", lambda: arrived(mb.reshape(8, 16, 512).at[pl.ds(0, 7)], mrecv))
-    mb[c, y] = pb[y]
+    mbf = mb.reshape(16, 16, 256)
+    led.expect("m out", lambda: arrived(mbf.at[pl.ds(0, 15)], msend))
+    led.expect("m", lambda: arrived(mbf.at[pl.ds(0, 15)], mrecv))
+    mb[c, side, y] = pb[side, y]
     led.wait("m")
-    sums = [mb[0, k].astype(F32) + mb[1, k].astype(F32) for k in range(4)]
     for zk in range(8):
-        at = (zk // 2) * 128
+        at = (zk // 4) * 128
         for h in range(2):
             cols = pl.ds(zk * 256 + h * 128, 128)
-            got = halves(sums[2 * h][:, at : at + 128], sums[2 * h + 1][:, at : at + 128], zk % 2)
-            am_ref[:, cols] = (tok[:, cols].astype(F32) + got).astype(BF16)
+            left, right = (
+                mb[0, zk % 2, k, :, at : at + 128].astype(F32) + mb[1, zk % 2, k, :, at : at + 128].astype(F32)
+                for k in (2 * h, 2 * h + 1)
+            )
+            am_ref[:, cols] = (tok[:, cols].astype(F32) + halves(left, right, zk // 2 % 2)).astype(BF16)
     rows = am_ref[...].astype(F32)
     scale = lax.rsqrt(jnp.mean(rows * rows, axis=-1, keepdims=True) + epsilon)
     ffn_in = (rows * scale * ffng[...]).astype(BF16)
@@ -347,7 +360,7 @@
         packed = jnp.dot(squeeze_rows(), zr[w].reshape(32, half), preferred_element_type=F32).astype(BF16)
         xg[w * 16 + u * 4 + v] = packed
         block = xg.at[w * 16 + u * 4 + v]
-        for k in (2, 1, 3):
+        for k in (1, 3, 2):
             remote(block, block, gsend, gu.at[w, u], plane_id(c, lines[k], v)).start()
         along_v(w, 0)
 
@@ -359,6 +372,13 @@
         led.wait(("rows", w, j, 1))
         rows_in = xg[pl.ds(w * 16 + lines[j] * 4, 4)].reshape(96, half)
         return jnp.dot(rows_in, wgu[halves_at[w], :], preferred_element_type=F32)
+
+    def reduce_v(w, j):
+        uj = lines[j]
+        for k in (2, 1, 3):
+            there = plane_id(c, u, across[k])
+            remote(po.at[w, uj, across[k]], pr.at[w, uj, v], psend, precv.at[w, uj], there).start()
+        led.expect(("part in", w, j), lambda: arrived(pr.at[w, uj, pl.ds(0, 3)], precv.at[w, uj]))
 
     def second(j):
         uj = lines[j]
@@ -368,10 +388,8 @@
         for w in range(2):
             part = jnp.dot(hidden, wd[:, halves_at[w]], preferred_element_type=F32).astype(BF16)
             po[w, uj] = part.reshape(4, 24, half)
-            for k in (2, 1, 3):
-                there = plane_id(c, u, across[k])
-                remote(po.at[w, uj, across[k]], pr.at[w, uj, v], psend, precv.at[w, uj], there).start()
-            led.expect(("part in", w, j), lambda w=w: arrived(pr.at[w, uj, pl.ds(0, 3)], precv.at[w, uj]))
+            if j:
+                reduce_v(w, j)
 
     def gather(w, j):
         uj = lines[j]
@@ -419,6 +437,8 @@
     second(3)
     second(1)
     second(2)
+    reduce_v(0, 0)
+    reduce_v(1, 0)
     for j in (3, 1, 2):
         for w in range(2):
             hand_over(w, j)
@@ -444,6 +464,22 @@
     led.finish()
 
 
+NPIECE = 4
+
+
+def emit_kernel(mixed_ref, state_ref, mixed_out, state_out, sem):
+    step = 16 // NPIECE
+    copies = [
+        pltpu.make_async_copy(state_ref.at[pl.ds(i * step, step)], state_out.at[pl.ds(i * step, step)], sem.at[i])
+        for i in range(NPIECE)
+    ]
+    copies.append(pltpu.make_async_copy(mixed_ref, mixed_out, sem.at[NPIECE]))
+    for copy in copies:
+        copy.start()
+    for copy in copies:
+        copy.wait()
+
+
 def shards(
     tokens, mix_gain, query_weight, forget_weight, input_weight, lower_bound, head_gain, out_weight, state,
     ffn_gain, route_ids, route_weights, expert_gate, expert_up, expert_down,
@@ -455,17 +491,18 @@
     dma = pltpu.SemaphoreType.DMA
     scratch = lambda *shape, dtype=BF16: pltpu.VMEM(shape, dtype)
     held = lambda a: pltpu.with_memory_space_constraint(a, pltpu.HBM)
-    return pl.pallas_call(
+    mixed_out, new_state = pl.pallas_call(
         layer_kernel,
-        out_shape=(jax.ShapeDtypeStruct((rows, half), BF16), pltpu.VMEM(state.shape, F32)),
+        out_shape=(pltpu.VMEM((rows, half), BF16), pltpu.VMEM(state.shape, F32)),
         in_specs=[hbm] * 15,
         out_specs=(vmem, vmem),
         scratch_shapes=[
             scratch(rows, width), scratch(1, width, dtype=F32), scratch(4, 128, dtype=F32), scratch(4, 128, dtype=F32),
             scratch(1, width, dtype=F32), scratch(2, 16, dtype=jnp.int32), scratch(2, 16, dtype=F32),
             scratch(4, 16, 384), scratch(8, 4, 16, 384), scratch(4, 16, 512), scratch(16, 16, 512),
-            scratch(16, 16, 384), scratch(16, 16, 384), scratch(16, 128, dtype=F32),
-            scratch(16, 512), scratch(8, 4, 16, 512), scratch(4, 16, 512), scratch(4, 16, 512), scratch(2, 4, 16, 512),
+            scratch(16, 16, 384), scratch(16, 16, 384), scratch(32, width), scratch(4, 16, 128, dtype=F32),
+            scratch(2, 4, 128, 32), scratch(4, 16, 128, dtype=F32),
+            scratch(16, 512), scratch(4, 4, 16, 512), scratch(2, 4, 16, 512), scratch(2, 4, 16, 256), scratch(2, 2, 4, 16, 256),
             scratch(rows, width), scratch(64, 16), scratch(64, 16, dtype=F32),
             scratch(width, 512), scratch(256, width), scratch(8, 8, width), scratch(2, 4, 8, half),
             scratch(32, 24, half), scratch(2, 4, 4, 24, half), scratch(2, 4, 4, 24, half), scratch(2, 4, 24, half),
@@ -485,6 +522,15 @@
             expert_gate, expert_up, expert_down,
         ))
     )
+    return pl.pallas_call(
+        emit_kernel,
+        out_shape=(pltpu.HBM(mixed_out.shape, BF16), pltpu.HBM(state.shape, F32)),
+        in_specs=[pl.BlockSpec(memory_space=pltpu.VMEM)] * 2,
+        out_specs=(hbm, hbm),
+        scratch_shapes=[dma((NPIECE + 1,))],
+        compiler_params=pltpu.CompilerParams(vmem_limit_bytes=4 * 2**20),
+        name="emit",
+    )(*(pltpu.with_memory_space_constraint(a, pltpu.VMEM) for a in (mixed_out, new_state)))
 
 
 def solution(mesh):

time: 82.9 us -> 79.8 us (0.963)
  local copies, waits for them, and re-layouts: 2.63 us -> 0 us
    unnamed x2 -> x0, local copies, waits for them, and re-layouts: 2.63 us -> none
    pallas_call x1 -> x2, Pallas kernels: 79.5 us -> 79.1 us  [the longest x1 77 us: shards(): pl.pallas_call(layer_kernel, out_shape=(pltpu.VMEM((rows, half), BF16), p...]
where the time goes in v4:
time: 79.8 us; the launch traced here: 79.7 us
  Pallas kernels  79.1 us (99%)
    pallas_call x1, Pallas kernels, shards(): pl.pallas_call(layer_kernel, out_shape=(pltpu.VMEM((rows, half), BF16), p...  77 us
    pallas_call x1, Pallas kernels, shards(): pl.pallas_call(emit_kernel, out_shape=(pltpu.HBM(mixed_out.shape, BF16),...  2.05 us

profile of v4, /device:TPU:1, one launch (start us, length us, event | category | flops | bytes accessed | tf_op | source)
XLA Modules:
  0.0 79.7 jit_solution(4485825944514885822)
XLA Ops:
  0.6 77.0 %layer.1 = (bf16[16,1024]{1,0:T(8,128)(2,1)S(1)}, f32[16,4,128,128]{3,2,1,0:T(8,128)S(1)}) custom-call(bf16[16,2048]{1,0:T(8,128)(2,1)} %tok_hbm.1, f32[1,2048]{1,0:T(1,128)} %bitcast.8, bf16[16,512]{1,0:T(8,128)(2,1)} %qw_hbm.1, bf16[16,512]{1,0:T(8,128)(2,1)} %fw_hbm.1, bf16[16,512]{1,0:T(8,128)(2,1)} %iw_hbm.1, f32[4,128]{1,0:T(4,128)} %bitcast.10, ...), custom_call_target="tpu_custom_call" | custom-call | tf_op jit(solution)/shard_map/layer/pallas_call | solution.py:494
  77.7 2.1 %emit.1 = (bf16[16,1024]{1,0:T(8,128)(2,1)}, f32[16,4,128,128]{3,2,1,0:T(8,128)}) custom-call(bf16[16,1024]{1,0:T(8,128)(2,1)S(1)} %get-tuple-element.4.mixed_ref, f32[16,4,128,128]{3,2,1,0:T(8,128)S(1)} %get-tuple-element.5.state_ref), custom_call_target="tpu_custom_call" | custom-call | tf_op jit(solution)/shard_map/emit/pallas_call | solution.py:525
